TPU v7x, 256 devices: a whole 4x4x8 slice. The times are simulated.
256 devices in a mesh: ep: 16 (over y, x), tp: 16 (over z, core).
Axes of the slice: x: 4, y: 4, z: 8, core: 2. Of those that a mesh axis runs over, the one named last changes fastest.
Arguments:
- queries: bfloat16 [12288, 2048], P('ep', 'tp'), may hold values from -6 to 6
- keys: bfloat16 [12288, 512], P('ep'), may hold values from -6 to 6
- values: bfloat16 [12288, 512], P('ep'), may hold values from -6 to 6
- query_gain: float32 [128], replicated, may hold values from 1 to 4.5
- key_gain: float32 [128], replicated, may hold values from 1 to 4.5
- out_weight: bfloat16 [2048, 2048], P('tp'), may hold values from -0.75 to 0.75
- tokens_b: bfloat16 [12288, 2048], P('ep'), may hold values from -6 to 6
- norm_gain: float32 [2048], replicated, may hold values from 0.1 to 1.9
- routes: int32 [12288, 2], P('ep'), may hold values from 0 to 15, all different within a row; in each aligned block of 48 rows (0 to 47, 48 to 95, ...) at most 8 rows name the same one
- route_weight: float32 [12288, 2], P('ep'), may hold values from 0.2 to 1
- gate_weight: bfloat16 [16, 2048, 4096], P('ep', None, 'tp'), may hold values from -0.125 to 0.125
- up_weight: bfloat16 [16, 2048, 4096], P('ep', None, 'tp'), may hold values from -0.125 to 0.125
- down_weight: bfloat16 [16, 4096, 2048], P('ep', 'tp'), may hold values from -0.09375 to 0.09375
Outputs:
- mixed_out: bfloat16 [12288, 2048], P(('ep', 'tp'))
- expert_out: bfloat16 [12288, 2048], P(('ep', 'tp'))
Inputs may be any that keep to these rules, and one draw needn't show every extreme that they name: `routes`: A row names 2 different experts. In each aligned block of 48 rows no expert is named more than 8 times, a bound that some block reaches.
All inputs are finite; a program needn't handle non-finite values.
Results may differ from a plain program's by a relative error of at most 0.019.
Values may be sent and summed in bfloat16 or wider, within the bound.
A program may use at most 128 MiB of HBM per device.

v0:
```python
import jax
import jax.numpy as jnp
from jax import lax
from jax.sharding import Mesh
from jax.sharding import PartitionSpec as P

D = 2048
HD = 128
HQ = 16
KVH = 4
EXPERTS = 16
TOPK = 2
GRID_W = 64
CAP = 8
TP = ("tp_0", "tp_1")
EP_TP = ("ep", "tp_0", "tp_1")


EPS = 1e-06
THETA = 10000.0


def side_by_side(arrays, axis, dim, along):
    ends, at = ([], 0)
    for a in arrays[:-1]:
        at += a.shape[along]
        ends.append(at)
    both = jnp.concatenate(arrays, axis=along)
    return tuple(jnp.split(lax.all_gather(both, axis, axis=dim, tiled=True), ends, axis=along))


def sum_in_order(blocks, axes, sequence):
    inside = blocks.shape[1:]
    blocks = blocks.reshape(*(lax.axis_size(a) for a in axes), *inside)
    blocks = jnp.moveaxis(blocks, sequence, range(len(axes))).reshape(-1, *inside)
    for k in sequence:
        blocks = lax.psum_scatter(blocks, axes[k], scatter_dimension=0, tiled=True)
    return blocks[0]


def split_up(x, dim, size):
    before, after = (x.shape[:dim], x.shape[dim + 1 :])
    return jnp.moveaxis(x.reshape(*before, size, -1, *after), dim, 0)


def scatter_axes(x, axes, sequence, dim):
    size = lax.axis_size(axes)
    return sum_in_order(split_up(x, dim, size), axes, sequence)


def rotate(field, positions):
    n_freq = HD // 4
    row_pos = (positions // GRID_W).astype(jnp.float32)
    col_pos = (positions % GRID_W).astype(jnp.float32)
    inverse = THETA ** (-jnp.arange(n_freq, dtype=jnp.float32) / n_freq)
    angles = jnp.stack([row_pos[:, None] * inverse, col_pos[:, None] * inverse], axis=1)
    cosine = jnp.cos(angles)[:, None]
    sine = jnp.sin(angles)[:, None]
    length, n_heads = (field.shape[0], field.shape[1])
    halves = field.reshape(length, n_heads, 2, 2, n_freq)
    leading = halves[..., 0, :]
    second = halves[..., 1, :]
    turned = jnp.stack(
        [leading * cosine - second * sine, second * cosine + leading * sine], axis=-2
    )
    return turned.reshape(length, n_heads, HD)


def prepare(source, gain_vec, positions, n_heads):
    length = source.shape[0]
    field = source.astype(jnp.float32).reshape(length, n_heads, HD)
    field = field * lax.rsqrt(jnp.mean(field * field, axis=-1, keepdims=True) + EPS) * gain_vec
    return rotate(field, positions).astype(jnp.bfloat16)


def token_mixer(queries, keys, values, query_gain, key_gain, out_weight):
    n_rows = queries.shape[0]
    q_heads = queries.shape[1] // HD
    positions = lax.axis_index("ep") * n_rows + jnp.arange(n_rows, dtype=jnp.int32)
    query_n = prepare(queries, query_gain, positions, q_heads).reshape(n_rows * q_heads, HD)
    kv_index = lax.axis_index(TP) * q_heads // (HQ // KVH)
    own_keys = prepare(
        lax.dynamic_slice_in_dim(keys, kv_index * HD, HD, 1), key_gain, positions, 1
    ).reshape(n_rows, HD)
    own_values = lax.dynamic_slice_in_dim(values, kv_index * HD, HD, 1)
    score_scale = HD ** (-0.5)
    start_state = (
        jnp.full((n_rows * q_heads,), -1e30, jnp.float32),
        jnp.zeros((n_rows * q_heads,), jnp.float32),
        jnp.zeros((n_rows * q_heads, HD), jnp.float32),
    )
    key_piece, value_piece = side_by_side((own_keys, own_values), "ep", 0, 1)
    steps_n = key_piece.shape[0] // n_rows

    def one_block(index_b, state):
        running_max, totals, numerator = state
        key_blk = lax.dynamic_slice_in_dim(key_piece, index_b * n_rows, n_rows, 0)
        value_blk = lax.dynamic_slice_in_dim(value_piece, index_b * n_rows, n_rows, 0)
        scores = (
            jnp.einsum("qd,sd->qs", query_n, key_blk, preferred_element_type=jnp.float32)
            * score_scale
        )
        new_max = jnp.maximum(running_max, jnp.max(scores, axis=1))
        shrink = jnp.exp(running_max - new_max)
        weights = jnp.exp(scores - new_max[:, None])
        totals = totals * shrink + jnp.sum(weights, axis=1)
        numerator = numerator * shrink[:, None] + jnp.dot(
            weights.astype(jnp.bfloat16), value_blk, preferred_element_type=jnp.float32
        )
        return (new_max, totals, numerator)

    running_max, totals, numerator = lax.fori_loop(0, steps_n, one_block, start_state)
    attended = (numerator / totals[:, None]).astype(jnp.bfloat16)
    own_rows = lax.all_to_all(attended, TP, split_axis=0, concat_axis=1, tiled=True)
    return jnp.dot(
        own_rows,
        lax.all_gather(out_weight, TP, axis=0, tiled=True),
        preferred_element_type=jnp.float32,
    ).astype(jnp.bfloat16)


def expert_half(tokens_b, norm_gain, routes, route_weight, gate_weight, up_weight, down_weight):
    n_tp = lax.axis_size(TP)
    n_ep = lax.axis_size("ep")
    tp_index = lax.axis_index(TP)
    local_rows = tokens_b.shape[0]
    block_rows = local_rows // n_tp
    picks = block_rows * TOPK
    local_experts = gate_weight.shape[0]
    assigned = routes.reshape(n_tp, picks)
    onehot = (assigned[:, :, None] == jnp.arange(EXPERTS, dtype=jnp.int32)[None, None, :]).astype(
        jnp.int32
    )
    slot_rank = jnp.sum((jnp.cumsum(onehot, axis=1) - onehot) * onehot, axis=-1)
    target = assigned * CAP + slot_rank
    target_hot = (
        target[:, :, None] == jnp.arange(EXPERTS * CAP, dtype=jnp.int32)[None, None, :]
    ).astype(jnp.float32)
    token_hot = (
        jnp.arange(picks, dtype=jnp.int32)[:, None] // TOPK
        == jnp.arange(block_rows, dtype=jnp.int32)[None, :]
    ).astype(jnp.float32)
    own_block = lax.dynamic_slice_in_dim(tokens_b, tp_index * block_rows, block_rows, 0)
    field = own_block.astype(jnp.float32)
    own_normed = (
        field * lax.rsqrt(jnp.mean(field * field, axis=-1, keepdims=True) + EPS) * norm_gain
    ).astype(jnp.bfloat16)
    own_hot = lax.dynamic_index_in_dim(target_hot, tp_index, 0, keepdims=False)
    own_mat = jnp.einsum("aj,at->jt", own_hot, token_hot, precision=lax.Precision.HIGHEST).astype(
        jnp.bfloat16
    )
    outgoing = jnp.dot(own_mat, own_normed, preferred_element_type=jnp.float32)
    outgoing = outgoing.astype(jnp.bfloat16).reshape(EXPERTS, CAP, D)
    arrived = lax.all_to_all(outgoing, "ep", split_axis=0, concat_axis=1, tiled=True)
    arrived = arrived.reshape(1, local_experts, n_ep * CAP, D)
    slab_rows = lax.all_gather(arrived, TP, axis=0, tiled=True)
    gate_act = jnp.einsum(
        "blmd,ldf->blmf", slab_rows, gate_weight, preferred_element_type=jnp.float32
    )
    up_act = jnp.einsum("blmd,ldf->blmf", slab_rows, up_weight, preferred_element_type=jnp.float32)
    hidden = (jax.nn.silu(gate_act) * up_act).astype(jnp.bfloat16)
    result = jnp.einsum("blmf,lfd->blmd", hidden, down_weight, preferred_element_type=jnp.float32)
    terms = result.reshape(-1, D)
    summed = (
        scatter_axes(terms.astype(jnp.bfloat16), TP, (1, 0), 0)
        .astype(jnp.float32)
        .astype(jnp.bfloat16)
    )
    returned = lax.all_to_all(
        summed.reshape(local_experts, n_ep, CAP, D), "ep", split_axis=1, concat_axis=0, tiled=True
    )
    returned = returned.reshape(EXPERTS * CAP, D)
    own_target = lax.dynamic_index_in_dim(target_hot, tp_index, 0, keepdims=False)
    shares = (route_weight / jnp.sum(route_weight, axis=-1, keepdims=True)).reshape(n_tp, picks)
    own_shares = lax.dynamic_index_in_dim(shares, tp_index, 0, keepdims=False)
    combine = jnp.einsum(
        "at,aj->tj", token_hot, own_target * own_shares[:, None], precision=lax.Precision.HIGHEST
    )
    return jnp.dot(combine, returned.astype(jnp.float32), precision=lax.Precision.HIGHEST).astype(
        jnp.bfloat16
    )


def on_device(
    queries,
    keys,
    values,
    query_gain,
    key_gain,
    out_weight,
    tokens_b,
    norm_gain,
    routes,
    route_weight,
    gate_weight,
    up_weight,
    down_weight,
):
    mixed_out = token_mixer(queries, keys, values, query_gain, key_gain, out_weight)
    expert_out = expert_half(
        tokens_b, norm_gain, routes, route_weight, gate_weight, up_weight, down_weight
    )
    return (mixed_out, expert_out)


def solution(mesh):
    torus = Mesh(mesh.devices.reshape(mesh.shape["ep"], 8, 2), ("ep", "tp_0", "tp_1"))
    in_specs = (
        P("ep", TP),
        P("ep", None),
        P("ep", None),
        P(),
        P(),
        P(TP, None),
        P("ep", None),
        P(),
        P("ep", None),
        P("ep", None),
        P("ep", None, TP),
        P("ep", None, TP),
        P("ep", TP, None),
    )
    out_specs = (P(EP_TP, None), P(EP_TP, None))
    return jax.shard_map(
        on_device, mesh=torus, in_specs=in_specs, out_specs=out_specs, check_vma=False
    )
```

profile of v0, /device:TPU:4, one launch (start us, length us, event | category | flops | bytes accessed | tf_op | source)
XLA Modules:
  0.0 288.9 jit_solution(9098463858573012935)
XLA Ops:
  8.1 1.0 copy.49
  9.4 2.1 select_reduce_fusion
  11.9 1.1 fusion.42
  13.3 1.3 fusion.16
  14.6 16.3 %all_to_all.37 = bf16[16,8,2048]{2,1,0:T(8,128)(2,1)} all-to-all(bf16[16,8,2048]{2,1,0:T(8,128)(2,1)S(1)} %fusion.16), channel_id=1, replica_groups=mesh['ep'=16,'tp_0'=8,'tp_1'=2] {'ep'}, dimensions={0} | all-to-all | bytes 1048576 | tf_op jit(solution)/shard_map/all_to_all | solution.py:154
  31.0 57.2 %all-gather.8.cloned.1.call-done = bf16[16,1,128,2048]{3,2,1,0:T(8,128)(2,1)} async-done(((bf16[1,1,128,2048]{3,2,1,0:T(8,128)(2,1)}), bf16[16,1,128,2048]{3,2,1,0:T(8,128)(2,1)}) %all-gather.8.cloned.1.call-update) | async-done | bytes 8388624 | tf_op jit(solution)/shard_map/all_gather | solution.py:156
  88.2 7.1 %fusion.14 = f32[16,128,256]{2,1,0:T(8,128)} fusion(bf16[16,1,128,2048]{3,2,1,0:T(8,128)(2,1)} %all-gather.8.cloned.1.call-done, bf16[1,2048,256]{2,1,0:T(8,128)(2,1)S(1)} %copy-done.7), kind=kOutput, calls=%fused_computation.20 | convolution fusion | flops 2147483648 | bytes 11534336 | tf_op jit(solution)/shard_map/blmd,ldf->blmf/dot_general | solution.py:157
  95.3 13.2 %convolution_convert_fusion = bf16[16,128,2048]{2,1,0:T(8,128)(2,1)} fusion(bf16[16,1,128,2048]{3,2,1,0:T(8,128)(2,1)} %all-gather.8.cloned.1.call-done, f32[16,128,256]{2,1,0:T(8,128)} %fusion.14, bf16[1,256,2048]{2,1,0:T(8,128)(2,1)S(1)} %copy-done, bf16[1,2048,256]{2,1,0:T(8,128)(2,1)S(1)} %copy-done.8), kind=kOutput, calls=%fused_computation.22 | convolution fusion | flops 4302307328 | bytes 20971520 | tf_op jit(solution)/shard_map/blmf,lfd->blmd/dot_general | solution.py:162
  108.5 8.3 %copy.53 = bf16[8,2,128,2048]{3,2,0,1:T(8,128)(2,1)} copy(bf16[8,2,128,2048]{3,2,1,0:T(8,128)(2,1)} %bitcast.112) | data formatting | bytes 16777216 | tf_op jit(solution)/shard_map/convert_element_type | solution.py:165
  116.9 1.1 constant_dynamic-slice_fusion.1
  118.9 0.8 subtract_convert_fusion
  119.7 0.8 pad_maximum_fusion
  120.6 16.8 %reduce-scatter.3.cloned.1.call-done = bf16[8,128,2048]{2,1,0:T(8,128)(2,1)} async-done(((bf16[16,128,2048]{2,1,0:T(8,128)(2,1)}), bf16[8,128,2048]{2,1,0:T(8,128)(2,1)}) %reduce-scatter.3.cloned.1.call-update) | async-done | bytes 4194320 | tf_op jit(solution)/shard_map/reduce_scatter | solution.py:37
  138.2 47.0 %all-gather.4.cloned.1.call-done = bf16[12288,256]{0,1:T(8,128)(2,1)} async-done(((bf16[768,256]{0,1:T(8,128)(2,1)}), bf16[12288,256]{0,1:T(8,128)(2,1)}) %all-gather.4.cloned.1.call-update) | async-done | bytes 6291472 | tf_op jit(solution)/shard_map/all_gather | solution.py:29
  185.2 6.2 %fusion.74 = (bf16[12288,128]{0,1:T(8,128)(2,1)}, bf16[12288,128]{0,1:T(8,128)(2,1)}) fusion(bf16[12288,256]{0,1:T(8,128)(2,1)} %all-gather.4.cloned.1.call-done), kind=kLoop, calls=%fused_computation.121 | loop fusion | bytes 12582912 | tf_op jit(solution)/shard_map/split | solution.py:29
  191.5 56.0 %while.18 = (s32[]{:T(128)}, f32[768]{0:T(1024)S(1)}, f32[768]{0:T(1024)S(1)}, f32[768,128]{1,0:T(8,128)S(1)}, bf16[12288,128]{0,1:T(8,128)(2,1)}, /*index=5*/bf...) while((s32[]{:T(128)}, f32[768]{0:T(1024)S(1)}, ...), condition=%wide.region_5.6_spmd.clone, body=%wide.region_2.5_spmd.clone.sunk | while | flops 307007232 | bytes 8503471 | solution.py:112
  191.5 1.4 multiply_reduce_fusion.2
  192.9 0.4 fusion.88
  193.4 1.6 convolution_add_fusion.2
  195.0 1.4 multiply_reduce_fusion.2
  196.4 0.4 fusion.88
  196.9 1.6 convolution_add_fusion.2
  198.4 1.4 multiply_reduce_fusion.2
  199.9 0.4 fusion.88
  200.3 1.6 convolution_add_fusion.2
  201.9 1.4 multiply_reduce_fusion.2
  203.8 1.6 convolution_add_fusion.2
  205.4 1.4 multiply_reduce_fusion.2
  206.9 0.4 fusion.88
  207.3 1.6 convolution_add_fusion.2
  208.9 1.4 multiply_reduce_fusion.2
  210.8 1.6 convolution_add_fusion.2
  212.5 1.4 multiply_reduce_fusion.2
  213.9 0.4 fusion.88
  214.4 1.6 convolution_add_fusion.2
  216.0 1.4 multiply_reduce_fusion.2
  217.4 0.4 fusion.88
  217.8 1.6 convolution_add_fusion.2
  219.5 1.4 multiply_reduce_fusion.2
  221.4 1.6 convolution_add_fusion.2
  223.0 1.4 multiply_reduce_fusion.2
  224.4 0.4 fusion.88
  224.9 1.6 convolution_add_fusion.2
  226.5 1.4 multiply_reduce_fusion.2
  228.0 0.4 fusion.88
  228.4 1.6 convolution_add_fusion.2
  230.0 1.4 multiply_reduce_fusion.2
  231.9 1.6 convolution_add_fusion.2
  233.5 1.4 multiply_reduce_fusion.2
  235.4 1.6 convolution_add_fusion.2
  237.0 1.4 multiply_reduce_fusion.2
  238.9 1.6 convolution_add_fusion.2
  240.5 1.4 multiply_reduce_fusion.2
  242.4 1.6 convolution_add_fusion.2
  244.0 1.4 multiply_reduce_fusion.2
  245.9 1.6 convolution_add_fusion.2
  247.5 0.9 divide_convert_fusion
  248.3 7.1 %all-to-all-start = ((bf16[16,48,128]{2,1,0:T(8,128)(2,1)}), bf16[16,48,128]{2,1,0:T(8,128)(2,1)S(1)}, u32[]{:S(2)}, u32[]{:S(2)}) async-start(bf16[16,48,128]{2,1,0:T(8,128)(2,1)} %bitcast.6), calls=%async_computation | async-start | bytes 393216 | tf_op jit(solution)/shard_map/all_to_all | solution.py:114
  255.8 1.0 fusion.54
  256.8 8.5 %all-to-all-done = bf16[16,48,128]{2,1,0:T(8,128)(2,1)S(1)} async-done(((bf16[16,48,128]{2,1,0:T(8,128)(2,1)}), bf16[16,48,128]{2,1,0:T(8,128)(2,1)S(1)}, u32[]{:S(2)}, u32[]{:S(2)}) %all-to-all-start) | async-done | bytes 196640 | tf_op jit(solution)/shard_map/all_to_all | solution.py:114
  265.3 5.7 %all-to-all-start.2 = ((bf16[1,16,8,2048]{3,2,0,1:T(8,128)(2,1)}), bf16[1,16,8,2048]{3,2,0,1:T(8,128)(2,1)S(1)}, u32[]{:S(2)}, u32[]{:S(2)}) async-start(bf16[1,16,8,2048]{3,2,0,1:T(8,128)(2,1)} %bitcast.118), calls=%async_computation.4 | async-start | bytes 1048576 | tf_op jit(solution)/shard_map/all_to_all | solution.py:169
  271.0 5.7 %convolution_convert_fusion.3 = bf16[48,2048]{1,0:T(8,128)(2,1)} fusion(bf16[2048,2048]{1,0:T(8,128)(2,1)} %all-gather.6.cloned.1.call-done, bf16[16,48,128]{2,1,0:T(8,128)(2,1)S(1)} %all-to-all-done), kind=kOutput, calls=%fused_computation.26 | convolution fusion | flops 402751488 | bytes 8781824 | tf_op jit(solution)/shard_map/dot_general | solution.py:115
  276.7 4.1 %all-to-all-done.2 = bf16[1,16,8,2048]{3,2,0,1:T(8,128)(2,1)S(1)} async-done(((bf16[1,16,8,2048]{3,2,0,1:T(8,128)(2,1)}), bf16[1,16,8,2048]{3,2,0,1:T(8,128)(2,1)S(1)}, u32[]{:S(2)}, u32[]{:S(2)}) %all-to-all-start.2) | async-done | bytes 524320 | tf_op jit(solution)/shard_map/all_to_all | solution.py:169
  280.8 1.0 convolution_convert_fusion.2
  (117 shorter events, 7.0 us)
Async XLA Ops:
  8.0 87.3 %copy-start = (bf16[1,256,2048]{2,1,0:T(8,128)(2,1)S(1)}, bf16[1,256,2048]{2,1,0:T(8,128)(2,1)}, u32[]{:S(2)}) copy-start(bf16[1,256,2048]{2,1,0:T(8,128)(2,1)} %param.27) | copy-start | bytes 3145732
  8.0 80.1 %copy-start.7 = (bf16[1,2048,256]{2,1,0:T(8,128)(2,1)S(1)}, bf16[1,2048,256]{2,1,0:T(8,128)(2,1)}, u32[]{:S(2)}) copy-start(bf16[1,2048,256]{2,1,0:T(8,128)(2,1)} %param.25) | copy-start | bytes 3145732
  8.0 80.1 %all-gather.8.cloned.1.call-start = ((), (), s32[]{:S(2)}) async-start(), calls=%async_computation.7 | async-start | bytes 8912896 | tf_op jit(solution)/shard_map/all_gather | solution.py:156
  11.9 83.4 %copy-start.3 = (pred[16,96,128]{2,1,0:T(32,128)(4,1)}, pred[16,96,128]{2,1,0:T(32,128)(4,1)S(1)}, u32[]{:S(2)}) copy-start(pred[16,96,128]{2,1,0:T(32,128)(4,1)S(1)} %iota_compare_fusion) | copy-start | bytes 589828
  30.9 64.4 %copy-start.8 = (bf16[1,2048,256]{2,1,0:T(8,128)(2,1)S(1)}, bf16[1,2048,256]{2,1,0:T(8,128)(2,1)}, u32[]{:S(2)}) copy-start(bf16[1,2048,256]{2,1,0:T(8,128)(2,1)} %param.26) | copy-start | bytes 3145732
  30.9 106.4 %reduce-scatter.3.cloned.1.call-start = ((), (), s32[]{:S(2)}) async-start(), calls=%async_computation.8 | async-start | bytes 12582912 | tf_op jit(solution)/shard_map/reduce_scatter | solution.py:37
  116.8 1.3 copy-start.2
  116.8 1.9 copy-start.5
  116.8 2.0 copy-start.6
  116.8 68.4 %all-gather.4.cloned.1.call-start = ((), (), s32[]{:S(2)}) async-start(), calls=%async_computation.5 | async-start | bytes 6684672 | tf_op jit(solution)/shard_map/all_gather | solution.py:29
  120.5 17.7 %copy-start.4 = (f32[768,2]{0,1:T(2,128)S(1)}, f32[768,2]{0,1:T(2,128)}, u32[]{:S(2)}) copy-start(f32[768,2]{0,1:T(2,128)} %param.24) | copy-start | bytes 18436
  120.5 144.8 %reduce-scatter.5.cloned.1.call-start = ((), (), s32[]{:S(2)}) async-start(), calls=%async_computation.9 | async-start | bytes 4718592 | tf_op jit(solution)/shard_map/reduce_scatter | solution.py:37
  137.4 133.6 %all-gather.6.cloned.1.call-start = ((), (), s32[]{:S(2)}) async-start(), calls=%async_computation.6 | async-start | bytes 8912896 | tf_op jit(solution)/shard_map/all_gather | solution.py:117
  248.3 16.9 %all-to-all-start = ((bf16[16,48,128]{2,1,0:T(8,128)(2,1)}), bf16[16,48,128]{2,1,0:T(8,128)(2,1)S(1)}, u32[]{:S(2)}, u32[]{:S(2)}) async-start(bf16[16,48,128]{2,1,0:T(8,128)(2,1)} %bitcast.6), calls=%async_computation | async-start | bytes 393216 | tf_op jit(solution)/shard_map/all_to_all | solution.py:114
  265.3 15.5 %all-to-all-start.2 = ((bf16[1,16,8,2048]{3,2,0,1:T(8,128)(2,1)}), bf16[1,16,8,2048]{3,2,0,1:T(8,128)(2,1)S(1)}, u32[]{:S(2)}, u32[]{:S(2)}) async-start(bf16[1,16,8,2048]{3,2,0,1:T(8,128)(2,1)} %bitcast.118), calls=%async_computation.4 | async-start | bytes 1048576 | tf_op jit(solution)/shard_map/all_to_all | solution.py:169
  271.0 10.8 %copy-start.1 = (bf16[1,256,2048]{2,1,0:T(8,128)(2,1)S(1)}, bf16[1,256,2048]{2,1,0:T(8,128)(2,1)}, u32[]{:S(2)}) copy-start(bf16[1,256,2048]{2,1,0:T(8,128)(2,1)} %param.27) | copy-start | bytes 3145732
Sparse Core Ops, SparseCore 0:
  31.0 57.0 all-gather.7
  116.9 20.3 reduce-scatter.2
  139.9 56.5 reduce-scatter.4
Sparse Core Ops, SparseCore 1:
  120.6 64.6 all-gather.3
  186.9 55.5 all-gather.5
where the time goes:
time: 293 us; the launch traced here: 289 us
  waiting for transfers between devices  134 us (46%)
  matrix products  77.7 us (27%)
  local copies, waits for them, and re-layouts  18 us (6%)
  blocking collectives  16.3 us (6%)
  between operations  15.5 us (5%)
  other arithmetic  13.6 us (5%)
  starting transfers between devices  13.1 us (4%)
    all_gather x1, waiting for transfers between devices, expert_half(): slab_rows = lax.all_gather(arrived, TP, axis=0, tiled=True)  57.2 us
    all_gather x1, waiting for transfers between devices, side_by_side(): lax.all_gather(both, axis, axis=dim, tiled=True)  47 us
    dot_general x16, matrix products, one_block(): jnp.dot(weights.astype(jnp.bfloat16), value_blk, preferred_element_type=j...  25.1 us
    dot_general x16, matrix products, one_block(): jnp.einsum('qd,sd->qs', query_n, key_blk, preferred_element_type=jnp.floa...  23 us
    reduce_scatter x2, waiting for transfers between devices, sum_in_order(): blocks = lax.psum_scatter(blocks, axes[k], scatter_dimension=0, tiled=True)  16.8 us
    all_to_all x1, blocking collectives, expert_half(): lax.all_to_all(outgoing, 'ep', split_axis=0, concat_axis=1, tiled=True)  16.3 us
    dot_general x1, matrix products, expert_half(): jnp.einsum('blmf,lfd->blmd', hidden, down_weight, preferred_element_type=...  13.2 us
    all_to_all x1, waiting for transfers between devices, token_mixer(): lax.all_to_all(attended, TP, split_axis=0, concat_axis=1, tiled=True)  8.45 us
  transfers between devices with their start and end apart: 7, of which 5 were waited for; matrix products, arithmetic and copies ran while one was open for 25% of the time, Pallas kernels for 0%

commit v1 on v0

v1 whole, which is shorter than its diff:
```python
import functools
import math

import jax
import jax.numpy as jnp
from jax import lax
from jax.experimental import pallas as pl
from jax.experimental.pallas import tpu as pltpu
from jax.sharding import Mesh
from jax.sharding import PartitionSpec as P

D = 2048
HD = 128
HQ = 16
KVH = 4
FF_DEV = 256
CAP = 8
GRID_W = 64
EPS = 1e-06
THETA = 10000.0

NX = 4
NY = 4
NE = NX * NY
NZ = 8
ROWS = 768
TOK = 48
CH = NE * CAP
HALF = CH // 2

REACH = 3
DIRECT = [0] + list(range(REACH + 1, NZ - REACH))
SUBS = 2
RSUBS = 2

MESH = pl.DeviceIdType.MESH
F32 = jnp.float32
BF16 = jnp.bfloat16

PLACES = [(0, 0)]
PLACES += [(0, 3), (0, 1), (3, 0), (1, 0)]
PLACES += [(3, 3), (3, 1), (1, 3), (1, 1), (0, 2), (2, 0)]
PLACES += [(3, 2), (1, 2), (2, 3), (2, 1)]
PLACES += [(2, 2)]
SLOT = {place: i for i, place in enumerate(PLACES)}
KEYS_UNIT = 2 * ROWS
UNITS = NE * ROWS // KEYS_UNIT
Q_TILE = 128


def gather_messages():
    out = []
    for half in (0, 1):
        base = half * (ROWS // 2)
        full, quarter = ROWS // 2, ROWS // 4
        prim, sec = ("x", "y") if half == 0 else ("y", "x")

        def slot(p, s, half=half):
            p, s = p % 4, s % 4
            return SLOT[(s, p)] if half == 0 else SLOT[(p, s)]

        def send(level, axis, step, p, s, part, half=half, base=base, full=full, quarter=quarter,
                 prim=prim, sec=sec, slot=slot):
            tp, ts = (p - step, s) if axis == prim else (p, s - step)
            start = base + (quarter if part == 1 else 0)
            rows = full if part is None else quarter
            out.append((level, half, axis, step, slot(p, s), slot(tp, ts), start, rows))

        for axis in (prim, sec):
            for step in (1, -1):
                send(1, axis, step, 0, 0, None)
        for p, step, part in ((-1, 1, 0), (1, -1, 1)):
            send(2, prim, step, p, 0, part)
            send(2, sec, 1, p, 0, None)
            send(2, sec, -1, p, 0, None)
        send(2, sec, 1, 0, -1, 0)
        send(2, sec, -1, 0, 1, 1)
        for p in (-1, 1):
            send(3, sec, 1, p, -1, 0)
            send(3, sec, -1, p, 1, 1)
        send(3, sec, 1, 2, 0, None)
        send(3, sec, -1, 2, 0, None)
        send(4, sec, 1, 2, -1, 0)
        send(4, sec, -1, 2, 1, 1)
    return sorted(out, key=lambda m: m[0])


MESSAGES = gather_messages()
N_MSG = len(MESSAGES)


def body(
    q_hbm, k_hbm, v_hbm, qg_ref, kg_ref, cr_ref, sr_ref, cc_ref, sc_ref, ng_ref,
    r0_ref, r1_ref, w0_ref, w1_ref, tok_hbm, ow_hbm, wg_hbm, wu_hbm, wd_hbm,
    mixed_ref, expert_ref,
    q_buf, kv_raw, tok_buf, kv, q_n, m_ref, acc_ref, att, att_sib, slots, rows,
    wg, wu, wd, ow, part, rs_buf, ap, ars_buf, fin, ret, mat_ref,
    in_sem, d2d_send, d2d_recv, kv_send, kv_recv, kvd_send, kvd_recv,
    a2a_send, a2a_recv, z_send, z_recv, rs_send, rs_recv, ars_send, ars_recv,
    ret_send, ret_recv,
):
    y = lax.axis_index("y")
    x = lax.axis_index("x")
    z = lax.axis_index("z")
    c = lax.axis_index("c")
    me = y * NX + x
    sib = 1 - c

    def remote(src, dst, send_sem, recv_sem, **device):
        return pltpu.make_async_remote_copy(
            src_ref=src, dst_ref=dst, send_sem=send_sem, recv_sem=recv_sem,
            device_id=device, device_id_type=MESH,
        )

    head = (2 * z + c) // 4
    lane = pl.ds(pl.multiple_of(head * HD, HD), HD)
    loads = [
        pltpu.make_async_copy(k_hbm.at[:, lane], kv_raw, in_sem.at[0]),
        pltpu.make_async_copy(v_hbm.at[:, lane], kv.at[1, 0], in_sem.at[1]),
        pltpu.make_async_copy(q_hbm, q_buf, in_sem.at[2]),
    ]
    for i, delta in enumerate(DIRECT):
        blk = (z + delta) % NZ * 2 + c
        loads.append(
            pltpu.make_async_copy(
                tok_hbm.at[pl.ds(pl.multiple_of(blk * TOK, TOK), TOK), :],
                tok_buf.at[i], in_sem.at[3 + i],
            )
        )
    for copy in loads:
        copy.start()
    weights = []
    for i, (src, dst) in enumerate(((wg_hbm, wg), (wu_hbm, wu), (wd_hbm, wd), (ow_hbm, ow))):
        weights.append(pltpu.make_async_copy(src, dst.at[c], in_sem.at[3 + len(DIRECT) + i]))
    for copy in weights:
        copy.start()

    def make_slots(i):
        delta = DIRECT[i]
        blk = (z + delta) % NZ * 2 + c
        loads[3 + i].wait()
        field = tok_buf[i].astype(F32)
        scale = lax.rsqrt(jnp.mean(field * field, axis=1, keepdims=True) + EPS)
        normed = (field * scale * ng_ref[...]).astype(BF16)
        j = lax.broadcasted_iota(jnp.int32, (CH, TOK), 0)
        expert, rank = j // CAP, j % CAP
        r0 = r0_ref[pl.ds(blk, 1), :]
        r1 = r1_ref[pl.ds(blk, 1), :]
        hot = ((r0 == expert) | (r1 == expert)).astype(F32)
        before = (
            lax.broadcasted_iota(jnp.int32, (TOK, TOK), 0)
            < lax.broadcasted_iota(jnp.int32, (TOK, TOK), 1)
        ).astype(BF16)
        count = jnp.dot(hot.astype(BF16), before, preferred_element_type=F32)
        mat = jnp.where(count == rank.astype(F32), hot, 0.0)
        if i == 0:
            mat_ref[...] = mat
        slots[i] = jnp.dot(mat.astype(BF16), normed, preferred_element_type=F32).astype(
            BF16
        ).reshape(NE, CAP, D)

    def a2a(i, j):
        dy, dx = PLACES[j]
        ty, tx = (y + dy) % NY, (x + dx) % NX
        return remote(
            slots.at[i, ty * NX + tx], rows.at[(z + DIRECT[i]) % NZ, me],
            a2a_send.at[i, j], a2a_recv.at[i, j], y=ty, x=tx,
        )

    def start_direct(i):
        for j in range(1, NE):
            a2a(i, j).start()
        rows[(z + DIRECT[i]) % NZ, me] = slots[i, me]

    def wait_direct(i):
        for j in range(1, NE):
            a2a(i, j).wait_recv()

    make_slots(0)
    start_direct(0)

    lane_of = lax.broadcasted_iota(jnp.int32, (GRID_W, HD), 1)
    pi = lax.broadcasted_iota(jnp.int32, (HD, HD), 0)
    pj = lax.broadcasted_iota(jnp.int32, (HD, HD), 1)
    first_half = pj % 64 < 32
    swap = jnp.where(
        first_half & (pi == pj + 32), -1.0, jnp.where(~first_half & (pi == pj - 32), 1.0, 0.0)
    ).astype(BF16)

    def turn(src, gain_ref, factor, store):
        gain = gain_ref[...]
        other = jnp.where(
            lax.broadcasted_iota(jnp.int32, (1, HD), 1) % 64 < 32,
            pltpu.roll(gain, HD - 32, 1), pltpu.roll(gain, 32, 1),
        )
        for g in range(ROWS // GRID_W):
            raw = src[g * GRID_W : (g + 1) * GRID_W, :]
            val = raw.astype(F32)
            inv = lax.rsqrt(jnp.mean(val * val, axis=1, keepdims=True) + EPS)
            if factor != 1.0:
                inv = inv * factor
            turned = jnp.dot(raw, swap, preferred_element_type=F32)
            cosine = jnp.where(lane_of < 64, cr_ref[g : g + 1, :], cc_ref[...])
            sine = jnp.where(lane_of < 64, sr_ref[g : g + 1, :], sc_ref[...])
            store(g, ((val * (gain * cosine) + turned * (other * sine)) * inv).astype(BF16))

    def store_key(g, val):
        kv[0, 0, g * GRID_W : (g + 1) * GRID_W, :] = val

    def store_query(g, val):
        q_n[g * GRID_W : (g + 1) * GRID_W, :] = val

    loads[0].wait()
    turn(kv_raw, kg_ref, 1.0, store_key)
    loads[1].wait()

    def kv_copy(n):
        _, _, axis, step, src, dst, start, size = MESSAGES[n]
        here = y if axis == "y" else x
        span = pl.ds(start, size)
        return remote(
            kv.at[c, src, span], kv.at[c, dst, span], kv_send.at[n], kv_recv.at[n],
            **{axis: (here + step) % 4},
        )

    def kv_across(slot, half):
        n = (slot - 1) * 2 + half
        span = pl.ds(half * (ROWS // 2), ROWS // 2)
        return remote(
            kv.at[c, slot, span], kv.at[c, slot, span], kvd_send.at[n], kvd_recv.at[n], c=sib
        )

    def kv_await(slot, half):
        n = (slot - 1) * 2 + half
        span = pl.ds(half * (ROWS // 2), ROWS // 2)
        return remote(
            kv.at[sib, slot, span], kv.at[sib, slot, span], kvd_send.at[n], kvd_recv.at[n], c=sib
        )

    for n, msg in enumerate(MESSAGES):
        if msg[0] == 1:
            kv_copy(n).start()

    def kv_level(level):
        done = {}
        for n, msg in enumerate(MESSAGES):
            if msg[0] != level:
                continue
            _, half, _, _, _, dst, _, size = msg
            kv_copy(n).wait_recv()
            done[dst, half] = done.get((dst, half), 0) + size
            if done[dst, half] == ROWS // 2:
                for k, later in enumerate(MESSAGES):
                    if later[0] == level + 1 and later[1] == half and later[4] == dst:
                        kv_copy(k).start()
                kv_across(dst, half).start()

    loads[2].wait()
    turn(q_buf, qg_ref, HD ** (-0.5) * math.log2(math.e), store_query)

    pairs = [
        remote(buf.at[c], buf.at[c], d2d_send.at[i], d2d_recv.at[i], c=sib)
        for i, buf in enumerate((wg, wu, wd, ow))
    ]
    awaited = [
        remote(buf.at[sib], buf.at[sib], d2d_send.at[i], d2d_recv.at[i], c=sib)
        for i, buf in enumerate((wg, wu, wd, ow))
    ]

    for i in range(1, len(DIRECT)):
        make_slots(i)

    def z_copy(way, hop, sub):
        step = 1 if way == 0 else -1
        chunk = (z - step * hop) % NZ
        span = pl.ds(sub * (NE // SUBS), NE // SUBS)
        return remote(
            rows.at[chunk, span], rows.at[chunk, span],
            z_send.at[way, hop, sub], z_recv.at[way, hop, sub], z=(z + step) % NZ,
        )

    def z_wait(way, hop, sub):
        step = 1 if way == 0 else -1
        chunk = (z - step * (hop + 1)) % NZ
        span = pl.ds(sub * (NE // SUBS), NE // SUBS)
        return remote(
            rows.at[chunk, span], rows.at[chunk, span],
            z_send.at[way, hop, sub], z_recv.at[way, hop, sub], z=(z + step) % NZ,
        )

    def z_start():
        wait_direct(0)
        for sub in range(SUBS):
            for way in (0, 1):
                z_copy(way, 0, sub).start()

    def z_forward(hop, sub):
        for way in (0, 1):
            z_wait(way, hop, sub).wait_recv()
            if hop + 1 < REACH:
                z_copy(way, hop + 1, sub).start()

    m_ref[...] = jnp.full_like(m_ref, -1e30)
    acc_ref[...] = jnp.zeros_like(acc_ref)

    hops = [(hop, sub) for hop in range(REACH) for sub in range(SUBS)]
    plan = {u: [] for u in range(UNITS + 1)}
    plan[0] += [z_start, functools.partial(kv_level, 1)]
    plan[2] += [functools.partial(kv_level, 2)]
    plan[4] += [functools.partial(kv_level, 3)]
    plan[6] += [functools.partial(kv_level, 4)]

    def send_weights():
        for i in range(4):
            weights[i].wait()
            pairs[i].start()

    plan[1] += [send_weights]
    for i in range(1, len(DIRECT)):
        plan[5] += [functools.partial(start_direct, i)]
    for k, at in enumerate((3, 5, 7)):
        if k < len(hops):
            plan[at] += [functools.partial(z_forward, *hops[k])]
    for hop in hops[3:]:
        plan[UNITS] += [functools.partial(z_forward, *hop)]

    def unit(u, carry):
        for k in range(UNITS):
            @pl.when(u == k)
            def _(k=k):
                for act in plan[k]:
                    act()
                for slot in (2 * k, 2 * k + 1):
                    if slot > 0:
                        for half in (0, 1):
                            kv_await(slot, half).wait_recv()

        keys = kv[0, pl.ds(2 * u, 2)].reshape(KEYS_UNIT, HD)
        vals = kv[1, pl.ds(2 * u, 2)].reshape(KEYS_UNIT, HD)
        wide = jnp.concatenate([vals, jnp.ones_like(vals)], axis=1)
        for i in range(ROWS // Q_TILE):
            sl = pl.ds(i * Q_TILE, Q_TILE)
            s = lax.dot_general(
                q_n[sl, :], keys, (((1,), (1,)), ((), ())), preferred_element_type=F32
            )
            old = m_ref[sl, :]
            new = jnp.maximum(old, jnp.max(s, axis=1, keepdims=True))
            shrink = jnp.exp2(old - new)
            p = jnp.exp2(s - new[:, :1]).astype(BF16)
            acc_ref[sl, :] = acc_ref[sl, :] * jnp.concatenate([shrink, shrink], axis=1) + jnp.dot(
                p, wide, preferred_element_type=F32
            )
            m_ref[sl, :] = new
        return carry

    lax.fori_loop(0, UNITS, unit, 0)
    for t in range(2 * NZ):
        span = pl.ds(t * TOK, TOK)
        att[t % 2, t // 2] = (acc_ref[span, :HD] / acc_ref[span, HD:]).astype(BF16)
    swap_att = remote(att.at[sib], att_sib, d2d_send.at[4], d2d_recv.at[4], c=sib)
    swap_att.start()
    for act in plan[UNITS]:
        act()
    for i in range(1, len(DIRECT)):
        wait_direct(i)
    for copy in awaited:
        copy.wait_recv()
    swap_att.wait_recv()

    piece = HALF // RSUBS

    def rs_copy(way, s, u):
        step = 1 if way == 0 else -1
        return remote(
            rs_buf.at[way, s, u], rs_buf.at[way, s + 1, u],
            rs_send.at[way, s, u], rs_recv.at[way, s, u], z=(z + step) % NZ,
        )

    def ars_copy(way, s):
        step = 1 if way == 0 else -1
        return remote(
            ars_buf.at[way, s], ars_buf.at[way, s + 1],
            ars_send.at[way, s], ars_recv.at[way, s], z=(z + step) % NZ,
        )

    def ret_copy(e):
        return remote(
            fin.at[e], ret.at[me], ret_send.at[e], ret_recv.at[me], y=e // NX, x=e % NX
        )

    def rs_step(s, carry):
        chunk_r = (z - 1 - s + 2 * NZ) % NZ
        chunk_l = (z + 1 + s) % NZ
        act = jnp.concatenate(
            [
                rows[chunk_r, 0 : NE // 2].reshape(HALF, D),
                rows[chunk_l, NE // 2 : NE].reshape(HALF, D),
            ],
            axis=0,
        )
        hidden = []
        for k in range(2):
            gate = jnp.dot(act, wg[k], preferred_element_type=F32)
            up = jnp.dot(act, wu[k], preferred_element_type=F32)
            hidden.append((gate / (1.0 + jnp.exp(-gate)) * up).astype(BF16))
        for k in range(4):
            cols = pl.ds(k * (D // 4), D // 4)
            part[:, cols] = jnp.dot(hidden[0], wd[0, :, cols], preferred_element_type=F32) + jnp.dot(
                hidden[1], wd[1, :, cols], preferred_element_type=F32
            )
        for way, chunk in ((0, chunk_r), (1, chunk_l)):
            cols = pl.ds(way * (D // 2), D // 2)
            ap[way] = jnp.dot(att[c, chunk], ow[c, :, cols], preferred_element_type=F32) + jnp.dot(
                att_sib[chunk], ow[sib, :, cols], preferred_element_type=F32
            )

        for u in range(RSUBS):
            for way in (0, 1):
                span = pl.ds(way * HALF + u * piece, piece)

                @pl.when(s == 0)
                def _(way=way, u=u, span=span):
                    rs_buf[way, 0, u] = part[span, :].astype(BF16)
                    rs_copy(way, 0, u).start()

                @pl.when(s > 0)
                def _(way=way, u=u, span=span):
                    rs_copy(way, s - 1, u).wait_recv()
                    total = part[span, :] + rs_buf[way, s, u].astype(F32)

                    @pl.when(s < NZ - 1)
                    def _():
                        rs_buf[way, s, u] = total.astype(BF16)
                        rs_copy(way, s, u).start()

                    @pl.when(s == NZ - 1)
                    def _():
                        count = piece // CAP
                        first = way * (NE // 2) + u * count
                        fin[pl.ds(first, count)] = total.astype(BF16).reshape(count, CAP, D)
                        for e in range(first, first + count):
                            @pl.when(me != e)
                            def _(e=e):
                                ret_copy(e).start()

        for way in (0, 1):
            @pl.when(s == 0)
            def _(way=way):
                ars_buf[way, 0] = ap[way].astype(BF16)
                ars_copy(way, 0).start()

            @pl.when(s > 0)
            def _(way=way):
                ars_copy(way, s - 1).wait_recv()
                total = ap[way] + ars_buf[way, s].astype(F32)

                @pl.when(s < NZ - 1)
                def _():
                    ars_buf[way, s] = total.astype(BF16)
                    ars_copy(way, s).start()

                @pl.when(s == NZ - 1)
                def _():
                    mixed_ref[:, way * (D // 2) : (way + 1) * (D // 2)] = total.astype(BF16)

        return carry

    lax.fori_loop(0, NZ, rs_step, 0)

    ret[me] = fin[me]
    own = 2 * z + c
    j = lax.broadcasted_iota(jnp.int32, (CH, TOK), 0)
    w0 = w0_ref[pl.ds(own, 1), :]
    w1 = w1_ref[pl.ds(own, 1), :]
    share = jnp.where(r0_ref[pl.ds(own, 1), :] == j // CAP, w0, w1) / (w0 + w1)
    combine = jnp.where(mat_ref[...] > 0.5, share, 0.0)
    high = combine.astype(BF16)
    low = (combine - high.astype(F32)).astype(BF16)
    for e in range(NE):
        @pl.when(me != e)
        def _(e=e):
            remote(
                fin.at[e], ret.at[e], ret_send.at[e], ret_recv.at[e], y=e // NX, x=e % NX
            ).wait_recv()
    back = ret[...].reshape(CH, D)
    dims = (((0,), (0,)), ((), ()))
    expert_ref[...] = (
        lax.dot_general(high, back, dims, preferred_element_type=F32)
        + lax.dot_general(low, back, dims, preferred_element_type=F32)
    ).astype(BF16)

    for e in range(NE):
        @pl.when(me != e)
        def _(e=e):
            ret_copy(e).wait_send()
    for n in range(N_MSG):
        kv_copy(n).wait_send()
    for slot in range(1, NE):
        for half in (0, 1):
            kv_across(slot, half).wait_send()
    for i in range(len(DIRECT)):
        for k in range(1, NE):
            a2a(i, k).wait_send()
    for copy in pairs:
        copy.wait_send()
    swap_att.wait_send()
    for way in (0, 1):
        for hop, sub in hops:
            z_copy(way, hop, sub).wait_send()
        for s in range(NZ - 1):
            for u in range(RSUBS):
                rs_copy(way, s, u).wait_send()
            ars_copy(way, s).wait_send()


def fused(*args):
    vmem = pl.BlockSpec(memory_space=pltpu.VMEM)
    hbm = pl.BlockSpec(memory_space=pl.ANY)
    dma = pltpu.SemaphoreType.DMA
    n_direct = len(DIRECT)
    return pl.pallas_call(
        body,
        name="fused_step",
        out_shape=(
            jax.ShapeDtypeStruct((TOK, D), BF16),
            jax.ShapeDtypeStruct((TOK, D), BF16),
        ),
        in_specs=[hbm] * 3 + [vmem] * 11 + [hbm] * 5,
        out_specs=(vmem, vmem),
        scratch_shapes=[
            pltpu.VMEM((ROWS, HD), BF16),
            pltpu.VMEM((ROWS, HD), BF16),
            pltpu.VMEM((n_direct, TOK, D), BF16),
            pltpu.VMEM((2, NE, ROWS, HD), BF16),
            pltpu.VMEM((ROWS, HD), BF16),
            pltpu.VMEM((ROWS, HD), F32),
            pltpu.VMEM((ROWS, 2 * HD), F32),
            pltpu.VMEM((2, NZ, TOK, HD), BF16),
            pltpu.VMEM((NZ, TOK, HD), BF16),
            pltpu.VMEM((n_direct, NE, CAP, D), BF16),
            pltpu.VMEM((NZ, NE, CAP, D), BF16),
            pltpu.VMEM((2, D, FF_DEV), BF16),
            pltpu.VMEM((2, D, FF_DEV), BF16),
            pltpu.VMEM((2, FF_DEV, D), BF16),
            pltpu.VMEM((2, HD, D), BF16),
            pltpu.VMEM((CH, D), F32),
            pltpu.VMEM((2, NZ, RSUBS, HALF // RSUBS, D), BF16),
            pltpu.VMEM((2, TOK, D // 2), F32),
            pltpu.VMEM((2, NZ, TOK, D // 2), BF16),
            pltpu.VMEM((NE, CAP, D), BF16),
            pltpu.VMEM((NE, CAP, D), BF16),
            pltpu.VMEM((CH, TOK), F32),
            dma((3 + n_direct + 4,)),
            dma((5,)), dma((5,)),
            dma((N_MSG,)), dma((N_MSG,)),
            dma((2 * NE - 2,)), dma((2 * NE - 2,)),
            dma((n_direct, NE)), dma((n_direct, NE)),
            dma((2, REACH, SUBS)), dma((2, REACH, SUBS)),
            dma((2, NZ, RSUBS)), dma((2, NZ, RSUBS)),
            dma((2, NZ)), dma((2, NZ)),
            dma((NE,)), dma((NE,)),
        ],
        compiler_params=pltpu.CompilerParams(
            has_side_effects=True, vmem_limit_bytes=60 * 2**20
        ),
    )(*args)


def on_device(
    queries, keys, values, query_gain, key_gain, out_weight, tokens_b, norm_gain,
    routes, route_weight, gate_weight, up_weight, down_weight,
):
    n_freq = HD // 4
    lane = jnp.arange(HD, dtype=jnp.int32) % n_freq
    inverse = (THETA ** (-jnp.arange(n_freq, dtype=F32) / n_freq))[lane][None, :]
    ep = lax.axis_index("y") * NX + lax.axis_index("x")
    grid_rows = ROWS // GRID_W
    row_pos = (ep * grid_rows + jnp.arange(grid_rows, dtype=jnp.int32)).astype(F32)[:, None]
    col_pos = jnp.arange(GRID_W, dtype=jnp.int32).astype(F32)[:, None]
    by_row, by_col = row_pos * inverse, col_pos * inverse
    blocks = 2 * NZ
    picks = jnp.moveaxis(routes.reshape(blocks, TOK, 2), 2, 0)
    sizes = jnp.moveaxis(route_weight.reshape(blocks, TOK, 2), 2, 0)
    return fused(
        queries, keys, values, query_gain[None, :], key_gain[None, :],
        jnp.cos(by_row), jnp.sin(by_row), jnp.cos(by_col), jnp.sin(by_col),
        norm_gain[None, :], picks[0], picks[1], sizes[0], sizes[1], tokens_b,
        out_weight, gate_weight[0], up_weight[0], down_weight[0],
    )


def solution(mesh):
    torus = Mesh(mesh.devices.reshape(NY, NX, NZ, 2), ("y", "x", "z", "c"))
    ep, tp = ("y", "x"), ("z", "c")
    in_specs = (
        P(ep, tp), P(ep, None), P(ep, None), P(), P(), P(tp, None), P(ep, None), P(),
        P(ep, None), P(ep, None), P(ep, None, tp), P(ep, None, tp), P(ep, tp, None),
    )
    out_specs = (P(ep + tp, None), P(ep + tp, None))
    return jax.shard_map(
        on_device, mesh=torus, in_specs=in_specs, out_specs=out_specs, check_vma=False
    )
```

time: 293 us -> 144 us (0.49)
  waiting for transfers between devices: 134 us -> 0 us
  Pallas kernels: 0 us -> 132 us
  matrix products: 77.7 us -> 0 us
  blocking collectives: 16.3 us -> 0 us
  between operations: 15.5 us -> 0.69 us
  starting transfers between devices: 13.1 us -> 0 us
  other arithmetic: 13.6 us -> 1.57 us
  local copies, waits for them, and re-layouts: 18 us -> 7.21 us
    pallas_call x0 -> x1, Pallas kernels: none -> 132 us  [fused(): pl.pallas_call(body, name='fused_step', out_shape=(jax.ShapeDtypeStruct((...]
    all_gather x3 -> x0, waiting for transfers between devices: 104 us -> none  [the longest x1 57.2 us: expert_half(): slab_rows = lax.all_gather(arrived, TP, axis=0, tiled=True)]
    dot_general x39 -> x0, matrix products: 77.7 us -> none  [the longest x16 25.1 us: one_block(): jnp.dot(weights.astype(jnp.bfloat16), value_blk, preferred_element_type=j...]
    reduce_scatter x2 -> x0, waiting for transfers between devices: 16.8 us -> none  [sum_in_order(): blocks = lax.psum_scatter(blocks, axes[k], scatter_dimension=0, tiled=True)]
    all_to_all x1 -> x0, blocking collectives: 16.3 us -> none  [expert_half(): lax.all_to_all(outgoing, 'ep', split_axis=0, concat_axis=1, tiled=True)]
    all_to_all x2 -> x0, starting transfers between devices: 12.7 us -> none  [the longest x1 7.05 us: token_mixer(): lax.all_to_all(attended, TP, split_axis=0, concat_axis=1, tiled=True)]
    all_to_all x2 -> x0, waiting for transfers between devices: 12.5 us -> none  [the longest x1 8.45 us: token_mixer(): lax.all_to_all(attended, TP, split_axis=0, concat_axis=1, tiled=True)]
    convert_element_type x1 -> x0, local copies, waits for them, and re-layouts: 8.27 us -> none  [expert_half(): terms.astype(jnp.bfloat16)]
  transfers between devices with their start and end apart: 7 -> 0, of which waited for: 5 -> 0; matrix products, arithmetic and copies ran while one was open for 25% -> 0% of each run, Pallas kernels for 0% -> 0%
where the time goes in v1:
time: 144 us; the launch traced here: 142 us
  Pallas kernels  132 us (92%)
  local copies, waits for them, and re-layouts  7.21 us (5%)
  other arithmetic  1.57 us (1%)
    pallas_call x1, Pallas kernels, fused(): pl.pallas_call(body, name='fused_step', out_shape=(jax.ShapeDtypeStruct((...  132 us
    unnamed x2, local copies, waits for them, and re-layouts  3.23 us

profile of v1, /device:TPU:4, one launch (start us, length us, event | category | flops | bytes accessed | tf_op | source)
XLA Modules:
  0.0 141.5 jit_solution(13093791797869273446)
XLA Ops:
  0.7 1.2 gather_fusion
  1.9 0.7 multiply_sine_fusion.1
  2.6 0.8 reshape.51
  3.4 0.6 slice_bitcast_fusion.2
  4.0 0.8 reshape.52
  4.8 0.6 slice_bitcast_fusion
  5.4 0.8 multiply_sine_fusion
  6.2 132.1 %fused_step.1 = (bf16[48,2048]{1,0:T(8,128)(2,1)}, bf16[48,2048]{1,0:T(8,128)(2,1)}) custom-call(bf16[768,128]{1,0:T(8,128)(2,1)} %q_hbm.1, bf16[768,512]{1,0:T(8,128)(2,1)} %k_hbm.1, bf16[768,512]{1,0:T(8,128)(2,1)} %v_hbm.1, f32[1,128]{1,0:T(1,128)} %bitcast.28, f32[1,128]{1,0:T(1,128)} %bitcast.29, f32[12,128]{1,0:T(8,128)} %get-tuple-element.9.cr_ref, ...), custom_call_target="tpu_custom_call" | custom-call | tf_op jit(solution)/shard_map/fused_step/pallas_call | solution.py:521
  138.3 1.6 %copy.17 = bf16[48,2048]{1,0:T(8,128)(2,1)} copy(bf16[48,2048]{1,0:T(8,128)(2,1)} %get-tuple-element.12) | data formatting | bytes 393216
  139.9 1.6 %copy.18 = bf16[48,2048]{1,0:T(8,128)(2,1)} copy(bf16[48,2048]{1,0:T(8,128)(2,1)} %get-tuple-element.13) | data formatting | bytes 393216
  (5 shorter events, 0.0 us)

commit v2 on v1

--- a/solution.py
+++ b/solution.py
@@ -3,6 +3,7 @@
 
 import jax
 import jax.numpy as jnp
+import numpy as np
 from jax import lax
 from jax.experimental import pallas as pl
 from jax.experimental.pallas import tpu as pltpu
@@ -28,10 +29,15 @@
 CH = NE * CAP
 HALF = CH // 2
 
-REACH = 3
+REACH = 2
 DIRECT = [0] + list(range(REACH + 1, NZ - REACH))
 SUBS = 2
 RSUBS = 2
+
+OWNERS = [(0, 2), (1, 2), (2, 0), (2, 1), (0, 0), (0, 1), (1, 0), (1, 1)]
+OWNERS += [(2, 2), (2, 3), (3, 1), (3, 2), (0, 3), (3, 0), (3, 3), (1, 3)]
+SELF = OWNERS.index((0, 0))
+OTHERS = [p for p in range(NE) if p != SELF]
 
 MESH = pl.DeviceIdType.MESH
 F32 = jnp.float32
@@ -45,6 +51,7 @@
 SLOT = {place: i for i, place in enumerate(PLACES)}
 KEYS_UNIT = 2 * ROWS
 UNITS = NE * ROWS // KEYS_UNIT
+EARLY = 6
 Q_TILE = 128
 
 
@@ -90,9 +97,9 @@
 
 
 def body(
-    q_hbm, k_hbm, v_hbm, qg_ref, kg_ref, cr_ref, sr_ref, cc_ref, sc_ref, ng_ref,
-    r0_ref, r1_ref, w0_ref, w1_ref, tok_hbm, ow_hbm, wg_hbm, wu_hbm, wd_hbm,
-    mixed_ref, expert_ref,
+    q_hbm, k_hbm, v_hbm, qg_ref, kg_ref, inv_ref, ng_ref, routes_ref, sizes_ref,
+    tok_hbm, ow_hbm, wg_hbm, wu_hbm, wd_hbm,
+    out_ref,
     q_buf, kv_raw, tok_buf, kv, q_n, m_ref, acc_ref, att, att_sib, slots, rows,
     wg, wu, wd, ow, part, rs_buf, ap, ars_buf, fin, ret, mat_ref,
     in_sem, d2d_send, d2d_recv, kv_send, kv_recv, kvd_send, kvd_recv,
@@ -111,6 +118,12 @@
             src_ref=src, dst_ref=dst, send_sem=send_sem, recv_sem=recv_sem,
             device_id=device, device_id_type=MESH,
         )
+
+    barrier = pltpu.get_barrier_semaphore()
+    partners = [{"y": (y + dy) % NY, "x": (x + dx) % NX} for dy, dx in PLACES[1:]]
+    partners += [{"z": (z + 1) % NZ}, {"z": (z + NZ - 1) % NZ}, {"c": sib}]
+    for partner in partners:
+        pl.semaphore_signal(barrier, inc=1, device_id=partner, device_id_type=MESH)
 
     head = (2 * z + c) // 4
     lane = pl.ds(pl.multiple_of(head * HD, HD), HD)
@@ -135,6 +148,9 @@
     for copy in weights:
         copy.start()
 
+    def block_of(ref, blk):
+        return pltpu.roll(ref[...], (ROWS - blk * TOK) % ROWS, 1)[:, :TOK]
+
     def make_slots(i):
         delta = DIRECT[i]
         blk = (z + delta) % NZ * 2 + c
@@ -144,8 +160,8 @@
         normed = (field * scale * ng_ref[...]).astype(BF16)
         j = lax.broadcasted_iota(jnp.int32, (CH, TOK), 0)
         expert, rank = j // CAP, j % CAP
-        r0 = r0_ref[pl.ds(blk, 1), :]
-        r1 = r1_ref[pl.ds(blk, 1), :]
+        picks = block_of(routes_ref, blk)
+        r0, r1 = picks[0:1], picks[1:2]
         hot = ((r0 == expert) | (r1 == expert)).astype(F32)
         before = (
             lax.broadcasted_iota(jnp.int32, (TOK, TOK), 0)
@@ -159,24 +175,26 @@
             BF16
         ).reshape(NE, CAP, D)
 
-    def a2a(i, j):
-        dy, dx = PLACES[j]
-        ty, tx = (y + dy) % NY, (x + dx) % NX
-        return remote(
-            slots.at[i, ty * NX + tx], rows.at[(z + DIRECT[i]) % NZ, me],
-            a2a_send.at[i, j], a2a_recv.at[i, j], y=ty, x=tx,
+    def a2a(i, p):
+        dy, dx = OWNERS[p]
+        ty, tx = (y - dy + NY) % NY, (x - dx + NX) % NX
+        return remote(
+            slots.at[i, ty * NX + tx], rows.at[(z + DIRECT[i]) % NZ, p],
+            a2a_send.at[i, p], a2a_recv.at[i, p], y=ty, x=tx,
         )
 
     def start_direct(i):
-        for j in range(1, NE):
-            a2a(i, j).start()
-        rows[(z + DIRECT[i]) % NZ, me] = slots[i, me]
-
-    def wait_direct(i):
-        for j in range(1, NE):
-            a2a(i, j).wait_recv()
+        for p in OTHERS:
+            a2a(i, p).start()
+        rows[(z + DIRECT[i]) % NZ, SELF] = slots[i, me]
+
+    def wait_direct(i, first=0, last=NE):
+        for p in OTHERS:
+            if first <= p < last:
+                a2a(i, p).wait_recv()
 
     make_slots(0)
+    pl.semaphore_wait(barrier, len(partners))
     start_direct(0)
 
     lane_of = lax.broadcasted_iota(jnp.int32, (GRID_W, HD), 1)
@@ -187,6 +205,13 @@
         first_half & (pi == pj + 32), -1.0, jnp.where(~first_half & (pi == pj - 32), 1.0, 0.0)
     ).astype(BF16)
 
+    row_pos = me * (ROWS // GRID_W) + lax.broadcasted_iota(jnp.int32, (16, HD), 0)
+    col_pos = lax.broadcasted_iota(jnp.int32, (GRID_W, HD), 0)
+    by_row = row_pos.astype(F32) * inv_ref[...]
+    by_col = col_pos.astype(F32) * inv_ref[...]
+    cos_row, sin_row = jnp.cos(by_row), jnp.sin(by_row)
+    cos_col, sin_col = jnp.cos(by_col), jnp.sin(by_col)
+
     def turn(src, gain_ref, factor, store):
         gain = gain_ref[...]
         other = jnp.where(
@@ -200,8 +225,8 @@
             if factor != 1.0:
                 inv = inv * factor
             turned = jnp.dot(raw, swap, preferred_element_type=F32)
-            cosine = jnp.where(lane_of < 64, cr_ref[g : g + 1, :], cc_ref[...])
-            sine = jnp.where(lane_of < 64, sr_ref[g : g + 1, :], sc_ref[...])
+            cosine = jnp.where(lane_of < 64, cos_row[g : g + 1, :], cos_col)
+            sine = jnp.where(lane_of < 64, sin_row[g : g + 1, :], sin_col)
             store(g, ((val * (gain * cosine) + turned * (other * sine)) * inv).astype(BF16))
 
     def store_key(g, val):
@@ -289,8 +314,8 @@
         )
 
     def z_start():
-        wait_direct(0)
         for sub in range(SUBS):
+            wait_direct(0, sub * (NE // SUBS), (sub + 1) * (NE // SUBS))
             for way in (0, 1):
                 z_copy(way, 0, sub).start()
 
@@ -306,25 +331,21 @@
     hops = [(hop, sub) for hop in range(REACH) for sub in range(SUBS)]
     plan = {u: [] for u in range(UNITS + 1)}
     plan[0] += [z_start, functools.partial(kv_level, 1)]
-    plan[2] += [functools.partial(kv_level, 2)]
-    plan[4] += [functools.partial(kv_level, 3)]
-    plan[6] += [functools.partial(kv_level, 4)]
-
     def send_weights():
         for i in range(4):
             weights[i].wait()
             pairs[i].start()
 
     plan[1] += [send_weights]
-    for i in range(1, len(DIRECT)):
-        plan[5] += [functools.partial(start_direct, i)]
-    for k, at in enumerate((3, 5, 7)):
-        if k < len(hops):
-            plan[at] += [functools.partial(z_forward, *hops[k])]
-    for hop in hops[3:]:
-        plan[UNITS] += [functools.partial(z_forward, *hop)]
-
-    def unit(u, carry):
+    plan[2] += [
+        functools.partial(z_forward, 0, 0), functools.partial(kv_level, 2),
+        functools.partial(z_forward, 0, 1),
+    ]
+    plan[4] += [functools.partial(kv_level, 3)]
+    plan[4] += [functools.partial(start_direct, i) for i in (1, 3)]
+    plan[6] += [functools.partial(kv_level, 4), functools.partial(start_direct, 2)]
+
+    def unit(u):
         for k in range(UNITS):
             @pl.when(u == k)
             def _(k=k):
@@ -351,21 +372,14 @@
                 p, wide, preferred_element_type=F32
             )
             m_ref[sl, :] = new
-        return carry
-
-    lax.fori_loop(0, UNITS, unit, 0)
-    for t in range(2 * NZ):
-        span = pl.ds(t * TOK, TOK)
-        att[t % 2, t // 2] = (acc_ref[span, :HD] / acc_ref[span, HD:]).astype(BF16)
+
     swap_att = remote(att.at[sib], att_sib, d2d_send.at[4], d2d_recv.at[4], c=sib)
-    swap_att.start()
-    for act in plan[UNITS]:
-        act()
-    for i in range(1, len(DIRECT)):
-        wait_direct(i)
-    for copy in awaited:
-        copy.wait_recv()
-    swap_att.wait_recv()
+
+    def finish_attention():
+        for t in range(2 * NZ):
+            span = pl.ds(t * TOK, TOK)
+            att[t % 2, t // 2] = (acc_ref[span, :HD] / acc_ref[span, HD:]).astype(BF16)
+        swap_att.start()
 
     piece = HALF // RSUBS
 
@@ -383,12 +397,27 @@
             ars_send.at[way, s], ars_recv.at[way, s], z=(z + step) % NZ,
         )
 
-    def ret_copy(e):
-        return remote(
-            fin.at[e], ret.at[me], ret_send.at[e], ret_recv.at[me], y=e // NX, x=e % NX
-        )
-
-    def rs_step(s, carry):
+    def ret_copy(p):
+        dy, dx = OWNERS[p]
+        return remote(
+            fin.at[p], ret.at[me], ret_send.at[p], ret_recv.at[p],
+            y=(y + dy) % NY, x=(x + dx) % NX,
+        )
+
+    def moe_step(s):
+        for k in range(NZ // 2):
+            @pl.when(s == k)
+            def _(k=k):
+                if k == 0:
+                    for copy in awaited:
+                        copy.wait_recv()
+                elif k < REACH:
+                    for sub in range(SUBS):
+                        z_forward(k, sub)
+                else:
+                    for delta in sorted({k + 1, NZ - k - 1}):
+                        wait_direct(DIRECT.index(delta))
+
         chunk_r = (z - 1 - s + 2 * NZ) % NZ
         chunk_l = (z + 1 + s) % NZ
         act = jnp.concatenate(
@@ -408,41 +437,47 @@
             part[:, cols] = jnp.dot(hidden[0], wd[0, :, cols], preferred_element_type=F32) + jnp.dot(
                 hidden[1], wd[1, :, cols], preferred_element_type=F32
             )
+        for u in range(RSUBS):
+            for way in (0, 1):
+                span = pl.ds(way * HALF + u * piece, piece)
+
+                @pl.when(s == 0)
+                def _(way=way, u=u, span=span):
+                    rs_buf[way, 0, u] = part[span, :].astype(BF16)
+                    rs_copy(way, 0, u).start()
+
+                @pl.when(s > 0)
+                def _(way=way, u=u, span=span):
+                    rs_copy(way, s - 1, u).wait_recv()
+                    total = part[span, :] + rs_buf[way, s, u].astype(F32)
+
+                    @pl.when(s < NZ - 1)
+                    def _():
+                        rs_buf[way, s, u] = total.astype(BF16)
+                        rs_copy(way, s, u).start()
+
+                    @pl.when(s == NZ - 1)
+                    def _():
+                        count = piece // CAP
+                        first = way * (NE // 2) + u * count
+                        fin[pl.ds(first, count)] = total.astype(BF16).reshape(count, CAP, D)
+                        for p in range(first, first + count):
+                            if p != SELF:
+                                ret_copy(p).start()
+
+    def att_step(s):
+        @pl.when(s == 0)
+        def _():
+            swap_att.wait_recv()
+
+        chunk_r = (z - 1 - s + 2 * NZ) % NZ
+        chunk_l = (z + 1 + s) % NZ
         for way, chunk in ((0, chunk_r), (1, chunk_l)):
             cols = pl.ds(way * (D // 2), D // 2)
             ap[way] = jnp.dot(att[c, chunk], ow[c, :, cols], preferred_element_type=F32) + jnp.dot(
                 att_sib[chunk], ow[sib, :, cols], preferred_element_type=F32
             )
 
-        for u in range(RSUBS):
-            for way in (0, 1):
-                span = pl.ds(way * HALF + u * piece, piece)
-
-                @pl.when(s == 0)
-                def _(way=way, u=u, span=span):
-                    rs_buf[way, 0, u] = part[span, :].astype(BF16)
-                    rs_copy(way, 0, u).start()
-
-                @pl.when(s > 0)
-                def _(way=way, u=u, span=span):
-                    rs_copy(way, s - 1, u).wait_recv()
-                    total = part[span, :] + rs_buf[way, s, u].astype(F32)
-
-                    @pl.when(s < NZ - 1)
-                    def _():
-                        rs_buf[way, s, u] = total.astype(BF16)
-                        rs_copy(way, s, u).start()
-
-                    @pl.when(s == NZ - 1)
-                    def _():
-                        count = piece // CAP
-                        first = way * (NE // 2) + u * count
-                        fin[pl.ds(first, count)] = total.astype(BF16).reshape(count, CAP, D)
-                        for e in range(first, first + count):
-                            @pl.when(me != e)
-                            def _(e=e):
-                                ret_copy(e).start()
-
         for way in (0, 1):
             @pl.when(s == 0)
             def _(way=way):
@@ -461,46 +496,58 @@
 
                 @pl.when(s == NZ - 1)
                 def _():
-                    mixed_ref[:, way * (D // 2) : (way + 1) * (D // 2)] = total.astype(BF16)
+                    out_ref[0, :, way * (D // 2) : (way + 1) * (D // 2)] = total.astype(BF16)
+
+    def tick(t, carry):
+        @pl.when(t < UNITS)
+        def _():
+            unit(t)
+
+        @pl.when(t == UNITS - 1)
+        def _():
+            finish_attention()
+
+        @pl.when((t == EARLY) | ((t >= UNITS) & (t < UNITS + NZ - 1)))
+        def _():
+            moe_step(jnp.where(t == EARLY, 0, t - UNITS + 1))
+
+        @pl.when(t >= UNITS)
+        def _():
+            att_step(t - UNITS)
 
         return carry
 
-    lax.fori_loop(0, NZ, rs_step, 0)
-
-    ret[me] = fin[me]
+    lax.fori_loop(0, UNITS + NZ, tick, 0)
+
+    ret[me] = fin[SELF]
     own = 2 * z + c
     j = lax.broadcasted_iota(jnp.int32, (CH, TOK), 0)
-    w0 = w0_ref[pl.ds(own, 1), :]
-    w1 = w1_ref[pl.ds(own, 1), :]
-    share = jnp.where(r0_ref[pl.ds(own, 1), :] == j // CAP, w0, w1) / (w0 + w1)
+    picks = block_of(routes_ref, own)
+    sizes = block_of(sizes_ref, own)
+    w0, w1 = sizes[0:1], sizes[1:2]
+    share = jnp.where(picks[0:1] == j // CAP, w0, w1) / (w0 + w1)
     combine = jnp.where(mat_ref[...] > 0.5, share, 0.0)
     high = combine.astype(BF16)
     low = (combine - high.astype(F32)).astype(BF16)
-    for e in range(NE):
-        @pl.when(me != e)
-        def _(e=e):
-            remote(
-                fin.at[e], ret.at[e], ret_send.at[e], ret_recv.at[e], y=e // NX, x=e % NX
-            ).wait_recv()
+    for p in OTHERS:
+        ret_copy(p).wait_recv()
     back = ret[...].reshape(CH, D)
     dims = (((0,), (0,)), ((), ()))
-    expert_ref[...] = (
+    out_ref[1] = (
         lax.dot_general(high, back, dims, preferred_element_type=F32)
         + lax.dot_general(low, back, dims, preferred_element_type=F32)
     ).astype(BF16)
 
-    for e in range(NE):
-        @pl.when(me != e)
-        def _(e=e):
-            ret_copy(e).wait_send()
+    for p in OTHERS:
+        ret_copy(p).wait_send()
     for n in range(N_MSG):
         kv_copy(n).wait_send()
     for slot in range(1, NE):
         for half in (0, 1):
             kv_across(slot, half).wait_send()
     for i in range(len(DIRECT)):
-        for k in range(1, NE):
-            a2a(i, k).wait_send()
+        for p in OTHERS:
+            a2a(i, p).wait_send()
     for copy in pairs:
         copy.wait_send()
     swap_att.wait_send()
@@ -521,12 +568,9 @@
     return pl.pallas_call(
         body,
         name="fused_step",
-        out_shape=(
-            jax.ShapeDtypeStruct((TOK, D), BF16),
-            jax.ShapeDtypeStruct((TOK, D), BF16),
-        ),
-        in_specs=[hbm] * 3 + [vmem] * 11 + [hbm] * 5,
-        out_specs=(vmem, vmem),
+        out_shape=jax.ShapeDtypeStruct((2, TOK, D), BF16),
+        in_specs=[hbm] * 3 + [vmem] * 6 + [hbm] * 5,
+        out_specs=vmem,
         scratch_shapes=[
             pltpu.VMEM((ROWS, HD), BF16),
             pltpu.VMEM((ROWS, HD), BF16),
@@ -561,7 +605,7 @@
             dma((NE,)), dma((NE,)),
         ],
         compiler_params=pltpu.CompilerParams(
-            has_side_effects=True, vmem_limit_bytes=60 * 2**20
+            collective_id=0, has_side_effects=True, vmem_limit_bytes=60 * 2**20
         ),
     )(*args)
 
@@ -571,22 +615,13 @@
     routes, route_weight, gate_weight, up_weight, down_weight,
 ):
     n_freq = HD // 4
-    lane = jnp.arange(HD, dtype=jnp.int32) % n_freq
-    inverse = (THETA ** (-jnp.arange(n_freq, dtype=F32) / n_freq))[lane][None, :]
-    ep = lax.axis_index("y") * NX + lax.axis_index("x")
-    grid_rows = ROWS // GRID_W
-    row_pos = (ep * grid_rows + jnp.arange(grid_rows, dtype=jnp.int32)).astype(F32)[:, None]
-    col_pos = jnp.arange(GRID_W, dtype=jnp.int32).astype(F32)[:, None]
-    by_row, by_col = row_pos * inverse, col_pos * inverse
-    blocks = 2 * NZ
-    picks = jnp.moveaxis(routes.reshape(blocks, TOK, 2), 2, 0)
-    sizes = jnp.moveaxis(route_weight.reshape(blocks, TOK, 2), 2, 0)
-    return fused(
-        queries, keys, values, query_gain[None, :], key_gain[None, :],
-        jnp.cos(by_row), jnp.sin(by_row), jnp.cos(by_col), jnp.sin(by_col),
-        norm_gain[None, :], picks[0], picks[1], sizes[0], sizes[1], tokens_b,
+    inverse = np.tile(THETA ** (-np.arange(n_freq) / n_freq), HD // n_freq).astype(np.float32)
+    both = fused(
+        queries, keys, values, query_gain[None, :], key_gain[None, :], jnp.asarray(inverse)[None, :],
+        norm_gain[None, :], routes.T, route_weight.T, tokens_b,
         out_weight, gate_weight[0], up_weight[0], down_weight[0],
     )
+    return both[0], both[1]
 
 
 def solution(mesh):

time: 144 us -> 111 us (0.77)
  Pallas kernels: 132 us -> 107 us
  local copies, waits for them, and re-layouts: 7.21 us -> 1.79 us
  other arithmetic: 1.57 us -> 0 us
    pallas_call x1, Pallas kernels: 132 us -> 107 us  [fused(): pl.pallas_call(body, name='fused_step', out_shape=jax.ShapeDtypeStruct((2...]
    unnamed x2 -> x0, local copies, waits for them, and re-layouts: 3.23 us -> none
    reshape x2 -> x0, local copies, waits for them, and re-layouts: 1.54 us -> none  [the longest x1 0.77 us: on_device(): picks = jnp.moveaxis(routes.reshape(blocks, TOK, 2), 2, 0)]
    sin x2 -> x0, other arithmetic: 1.54 us -> none  [the longest x1 0.82 us: on_device(): jnp.sin(by_col)]
where the time goes in v2:
time: 111 us; the launch traced here: 109 us
  Pallas kernels  107 us (96%)
  local copies, waits for them, and re-layouts  1.79 us (2%)
    pallas_call x1, Pallas kernels, fused(): pl.pallas_call(body, name='fused_step', out_shape=jax.ShapeDtypeStruct((2...  107 us

profile of v2, /device:TPU:4, one launch (start us, length us, event | category | flops | bytes accessed | tf_op | source)
XLA Modules:
  0.0 109.5 jit_solution(4878751656128132056)
XLA Ops:
  0.6 107.0 %fused_step.1 = bf16[2,48,2048]{2,1,0:T(8,128)(2,1)} custom-call(bf16[768,128]{1,0:T(8,128)(2,1)} %q_hbm.1, bf16[768,512]{1,0:T(8,128)(2,1)} %k_hbm.1, bf16[768,512]{1,0:T(8,128)(2,1)} %v_hbm.1, f32[1,128]{1,0:T(1,128)} %bitcast.18, f32[1,128]{1,0:T(1,128)} %bitcast.19, f32[1,128]{1,0:T(1,128)} %constant.6.inv_ref, f32[1,2048]{1,0:T(1,128)} %bitcast.15, ...), custom_call_target="tpu_custom_call" | custom-call | tf_op jit(solution)/shard_map/fused_step/pallas_call | solution.py:568
  107.7 1.8 %slice_bitcast_fusion = (bf16[48,2048]{1,0:T(8,128)(2,1)}, bf16[48,2048]{1,0:T(8,128)(2,1)}) fusion(bf16[2,48,2048]{2,1,0:T(8,128)(2,1)} %fused_step.1), kind=kLoop, calls=%fused_computation | loop fusion | bytes 786432 | tf_op jit(solution)/shard_map/squeeze | solution.py:624

commit v3 on v2

--- a/solution.py
+++ b/solution.py
@@ -31,13 +31,16 @@
 
 REACH = 2
 DIRECT = [0] + list(range(REACH + 1, NZ - REACH))
-SUBS = 2
+SUBS = 4
+PIECE = NE // SUBS
+SUB_ORDER = (1, 3, 0, 2)
 RSUBS = 2
 
 OWNERS = [(0, 2), (1, 2), (2, 0), (2, 1), (0, 0), (0, 1), (1, 0), (1, 1)]
 OWNERS += [(2, 2), (2, 3), (3, 1), (3, 2), (0, 3), (3, 0), (3, 3), (1, 3)]
 SELF = OWNERS.index((0, 0))
 OTHERS = [p for p in range(NE) if p != SELF]
+NEAR_FIRST = [p for sub in SUB_ORDER for p in range(sub * PIECE, (sub + 1) * PIECE) if p != SELF]
 
 MESH = pl.DeviceIdType.MESH
 F32 = jnp.float32
@@ -51,7 +54,9 @@
 SLOT = {place: i for i, place in enumerate(PLACES)}
 KEYS_UNIT = 2 * ROWS
 UNITS = NE * ROWS // KEYS_UNIT
-EARLY = 6
+EARLY = (4, 6)
+TICKS = UNITS + NZ - len(EARLY)
+WO_ROWS = NZ * HD
 Q_TILE = 128
 
 
@@ -100,11 +105,10 @@
     q_hbm, k_hbm, v_hbm, qg_ref, kg_ref, inv_ref, ng_ref, routes_ref, sizes_ref,
     tok_hbm, ow_hbm, wg_hbm, wu_hbm, wd_hbm,
     out_ref,
-    q_buf, kv_raw, tok_buf, kv, q_n, m_ref, acc_ref, att, att_sib, slots, rows,
-    wg, wu, wd, ow, part, rs_buf, ap, ars_buf, fin, ret, mat_ref,
-    in_sem, d2d_send, d2d_recv, kv_send, kv_recv, kvd_send, kvd_recv,
-    a2a_send, a2a_recv, z_send, z_recv, rs_send, rs_recv, ars_send, ars_recv,
-    ret_send, ret_recv,
+    q_buf, kv_raw, tok_buf, kv, q_n, m_ref, acc_ref, att, slots, rows,
+    wg, wu, wd, wo, att_all, part, rs_buf, fin, ret, mat_ref, comb, stage,
+    in_sem, d2d_send, d2d_recv, sent, a2a_sent, ring_sent, kv_recv, kvd_recv, a2a_recv, z_recv,
+    wo_recv, wod_recv, rs_recv, out_sem,
 ):
     y = lax.axis_index("y")
     x = lax.axis_index("x")
@@ -121,9 +125,12 @@
 
     barrier = pltpu.get_barrier_semaphore()
     partners = [{"y": (y + dy) % NY, "x": (x + dx) % NX} for dy, dx in PLACES[1:]]
-    partners += [{"z": (z + 1) % NZ}, {"z": (z + NZ - 1) % NZ}, {"c": sib}]
+    partners += [{"z": (z + dz) % NZ} for dz in range(1, NZ)]
+    partners += [{"z": (z + dz) % NZ, "c": sib} for dz in range(NZ)]
     for partner in partners:
         pl.semaphore_signal(barrier, inc=1, device_id=partner, device_id_type=MESH)
+
+    outs = [pltpu.make_async_copy(stage.at[i], out_ref.at[i], out_sem.at[i]) for i in range(2)]
 
     head = (2 * z + c) // 4
     lane = pl.ds(pl.multiple_of(head * HD, HD), HD)
@@ -143,8 +150,12 @@
     for copy in loads:
         copy.start()
     weights = []
-    for i, (src, dst) in enumerate(((wg_hbm, wg), (wu_hbm, wu), (wd_hbm, wd), (ow_hbm, ow))):
+    for i, (src, dst) in enumerate(((wg_hbm, wg), (wu_hbm, wu), (wd_hbm, wd))):
         weights.append(pltpu.make_async_copy(src, dst.at[c], in_sem.at[3 + len(DIRECT) + i]))
+    slab = pl.ds(pl.multiple_of(me * HD, HD), HD)
+    wo_own = wo.at[c, 0, pl.ds(pl.multiple_of(z * HD, HD), HD)]
+    wo_load = pltpu.make_async_copy(ow_hbm.at[:, slab], wo_own, in_sem.at[6 + len(DIRECT)])
+    wo_load.start()
     for copy in weights:
         copy.start()
 
@@ -180,22 +191,38 @@
         ty, tx = (y - dy + NY) % NY, (x - dx + NX) % NX
         return remote(
             slots.at[i, ty * NX + tx], rows.at[(z + DIRECT[i]) % NZ, p],
-            a2a_send.at[i, p], a2a_recv.at[i, p], y=ty, x=tx,
+            a2a_sent.at[i], a2a_recv.at[p // PIECE if i == 0 else SUBS + i - 1], y=ty, x=tx,
         )
 
     def start_direct(i):
-        for p in OTHERS:
+        for p in NEAR_FIRST:
             a2a(i, p).start()
         rows[(z + DIRECT[i]) % NZ, SELF] = slots[i, me]
 
-    def wait_direct(i, first=0, last=NE):
-        for p in OTHERS:
-            if first <= p < last:
-                a2a(i, p).wait_recv()
+    def wait_rows(i, sem, first, count):
+        span = rows.at[(z + DIRECT[i]) % NZ, pl.ds(first, count)]
+        remote(span, span, a2a_sent.at[i], a2a_recv.at[sem], c=sib).wait_recv()
+
+    def wait_own(sub):
+        wait_rows(0, sub, sub * PIECE, PIECE - (SELF // PIECE == sub))
+
+    def wait_direct(i):
+        wait_rows(i, SUBS + i - 1, 0, NE - 1)
 
     make_slots(0)
     pl.semaphore_wait(barrier, len(partners))
     start_direct(0)
+
+    own = 2 * z + c
+    j = lax.broadcasted_iota(jnp.int32, (CH, TOK), 0)
+    picks = block_of(routes_ref, own)
+    sizes = block_of(sizes_ref, own)
+    w0, w1 = sizes[0:1], sizes[1:2]
+    share = jnp.where(picks[0:1] == j // CAP, w0, w1) / (w0 + w1)
+    combine = jnp.where(mat_ref[...] > 0.5, share, 0.0)
+    high = combine.astype(BF16)
+    comb[0] = high
+    comb[1] = (combine - high.astype(F32)).astype(BF16)
 
     lane_of = lax.broadcasted_iota(jnp.int32, (GRID_W, HD), 1)
     pi = lax.broadcasted_iota(jnp.int32, (HD, HD), 0)
@@ -239,57 +266,68 @@
     turn(kv_raw, kg_ref, 1.0, store_key)
     loads[1].wait()
 
-    def kv_copy(n):
-        _, _, axis, step, src, dst, start, size = MESSAGES[n]
-        here = y if axis == "y" else x
-        span = pl.ds(start, size)
-        return remote(
-            kv.at[c, src, span], kv.at[c, dst, span], kv_send.at[n], kv_recv.at[n],
-            **{axis: (here + step) % 4},
-        )
-
-    def kv_across(slot, half):
-        n = (slot - 1) * 2 + half
-        span = pl.ds(half * (ROWS // 2), ROWS // 2)
-        return remote(
-            kv.at[c, slot, span], kv.at[c, slot, span], kvd_send.at[n], kvd_recv.at[n], c=sib
-        )
-
-    def kv_await(slot, half):
-        n = (slot - 1) * 2 + half
-        span = pl.ds(half * (ROWS // 2), ROWS // 2)
-        return remote(
-            kv.at[sib, slot, span], kv.at[sib, slot, span], kvd_send.at[n], kvd_recv.at[n], c=sib
-        )
-
-    for n, msg in enumerate(MESSAGES):
-        if msg[0] == 1:
-            kv_copy(n).start()
-
-    def kv_level(level):
-        done = {}
-        for n, msg in enumerate(MESSAGES):
-            if msg[0] != level:
-                continue
-            _, half, _, _, _, dst, _, size = msg
-            kv_copy(n).wait_recv()
-            done[dst, half] = done.get((dst, half), 0) + size
-            if done[dst, half] == ROWS // 2:
+    class Gather:
+        def __init__(self, buf, size, first, arrived, crossed):
+            self.buf, self.size, self.arrived, self.crossed = buf, size, arrived, crossed
+            self.ring, self.across_sem = sent.at[first], sent.at[first + 1]
+
+        def copy(self, n):
+            _, half, axis, step, src, dst, start, count = MESSAGES[n]
+            here = y if axis == "y" else x
+            span = pl.ds(start * self.size // ROWS, count * self.size // ROWS)
+            return remote(
+                self.buf.at[c, src, span], self.buf.at[c, dst, span], self.ring,
+                self.arrived.at[(dst - 1) * 2 + half], **{axis: (here + step) % 4},
+            )
+
+        def start(self):
+            for n, msg in enumerate(MESSAGES):
+                if msg[0] == 1:
+                    self.copy(n).start()
+
+        def level(self, level):
+            for dst, half in dict.fromkeys((m[5], m[1]) for m in MESSAGES if m[0] == level):
+                span = self.buf.at[c, dst, pl.ds(half * (self.size // 2), self.size // 2)]
+                remote(span, span, self.ring, self.arrived.at[(dst - 1) * 2 + half], c=sib).wait_recv()
                 for k, later in enumerate(MESSAGES):
                     if later[0] == level + 1 and later[1] == half and later[4] == dst:
-                        kv_copy(k).start()
-                kv_across(dst, half).start()
+                        self.copy(k).start()
+                remote(span, span, self.across_sem, self.crossed.at[dst // 2], c=sib).start()
+
+        def wait(self, pair):
+            first = max(2 * pair, 1)
+            span = self.buf.at[sib, pl.ds(first, 2 * pair + 2 - first)]
+            remote(span, span, self.across_sem, self.crossed.at[pair], c=sib).wait_recv()
+
+    kvs = Gather(kv, ROWS, 0, kv_recv, kvd_recv)
+    wos = Gather(wo, WO_ROWS, 5, wo_recv, wod_recv)
+    kv_level = kvs.level
+    kvs.start()
+
+    def wo_copy(dz):
+        return remote(wo_own, wo_own, sent.at[7], sent.at[8], z=(z + dz) % NZ)
+
+    wo_load.wait()
+    for dz in range(1, NZ):
+        wo_copy(dz).start()
+
+    def wo_start():
+        span = wo.at[c, 0, pl.ds(0, WO_ROWS - HD)]
+        remote(span, span, sent.at[7], sent.at[8], c=sib).wait_recv()
+        own = wo.at[c, 0]
+        remote(own, own, d2d_send.at[3], d2d_recv.at[3], c=sib).start()
+        wos.start()
 
     loads[2].wait()
     turn(q_buf, qg_ref, HD ** (-0.5) * math.log2(math.e), store_query)
 
     pairs = [
         remote(buf.at[c], buf.at[c], d2d_send.at[i], d2d_recv.at[i], c=sib)
-        for i, buf in enumerate((wg, wu, wd, ow))
+        for i, buf in enumerate((wg, wu, wd))
     ]
     awaited = [
         remote(buf.at[sib], buf.at[sib], d2d_send.at[i], d2d_recv.at[i], c=sib)
-        for i, buf in enumerate((wg, wu, wd, ow))
+        for i, buf in enumerate((wg, wu, wd))
     ]
 
     for i in range(1, len(DIRECT)):
@@ -298,24 +336,24 @@
     def z_copy(way, hop, sub):
         step = 1 if way == 0 else -1
         chunk = (z - step * hop) % NZ
-        span = pl.ds(sub * (NE // SUBS), NE // SUBS)
+        span = pl.ds(sub * PIECE, PIECE)
         return remote(
             rows.at[chunk, span], rows.at[chunk, span],
-            z_send.at[way, hop, sub], z_recv.at[way, hop, sub], z=(z + step) % NZ,
+            sent.at[2], z_recv.at[way, hop, sub], z=(z + step) % NZ,
         )
 
     def z_wait(way, hop, sub):
         step = 1 if way == 0 else -1
         chunk = (z - step * (hop + 1)) % NZ
-        span = pl.ds(sub * (NE // SUBS), NE // SUBS)
+        span = pl.ds(sub * PIECE, PIECE)
         return remote(
             rows.at[chunk, span], rows.at[chunk, span],
-            z_send.at[way, hop, sub], z_recv.at[way, hop, sub], z=(z + step) % NZ,
+            sent.at[2], z_recv.at[way, hop, sub], z=(z + step) % NZ,
         )
 
     def z_start():
-        for sub in range(SUBS):
-            wait_direct(0, sub * (NE // SUBS), (sub + 1) * (NE // SUBS))
+        for sub in SUB_ORDER:
+            wait_own(sub)
             for way in (0, 1):
                 z_copy(way, 0, sub).start()
 
@@ -332,18 +370,18 @@
     plan = {u: [] for u in range(UNITS + 1)}
     plan[0] += [z_start, functools.partial(kv_level, 1)]
     def send_weights():
-        for i in range(4):
+        for i in range(3):
             weights[i].wait()
             pairs[i].start()
 
-    plan[1] += [send_weights]
-    plan[2] += [
-        functools.partial(z_forward, 0, 0), functools.partial(kv_level, 2),
-        functools.partial(z_forward, 0, 1),
-    ]
-    plan[4] += [functools.partial(kv_level, 3)]
-    plan[4] += [functools.partial(start_direct, i) for i in (1, 3)]
-    plan[6] += [functools.partial(kv_level, 4), functools.partial(start_direct, 2)]
+    forward = [functools.partial(z_forward, 0, sub) for sub in SUB_ORDER]
+    plan[0] += [forward[0]]
+    plan[1] += [forward[1], send_weights]
+    plan[2] += [forward[2], forward[3], functools.partial(kv_level, 2)]
+    plan[2] += [functools.partial(start_direct, 1)]
+    plan[4] += [functools.partial(kv_level, 3), functools.partial(start_direct, 3)]
+    plan[6] += [functools.partial(kv_level, 4), functools.partial(start_direct, 2), wo_start]
+    late = {UNITS: 1, UNITS + 2: 2, UNITS + 3: 3, UNITS + 4: 4}
 
     def unit(u):
         for k in range(UNITS):
@@ -351,10 +389,7 @@
             def _(k=k):
                 for act in plan[k]:
                     act()
-                for slot in (2 * k, 2 * k + 1):
-                    if slot > 0:
-                        for half in (0, 1):
-                            kv_await(slot, half).wait_recv()
+                kvs.wait(k)
 
         keys = kv[0, pl.ds(2 * u, 2)].reshape(KEYS_UNIT, HD)
         vals = kv[1, pl.ds(2 * u, 2)].reshape(KEYS_UNIT, HD)
@@ -373,13 +408,22 @@
             )
             m_ref[sl, :] = new
 
-    swap_att = remote(att.at[sib], att_sib, d2d_send.at[4], d2d_recv.at[4], c=sib)
+    def att_copy(dz, core):
+        to = (z + dz) % NZ
+        head = pl.ds(pl.multiple_of(z * HD, HD), HD)
+        return remote(
+            att.at[core * NZ + to], att_all.at[c, :, head], sent.at[9], sent.at[10], z=to, c=core
+        )
 
     def finish_attention():
         for t in range(2 * NZ):
             span = pl.ds(t * TOK, TOK)
-            att[t % 2, t // 2] = (acc_ref[span, :HD] / acc_ref[span, HD:]).astype(BF16)
-        swap_att.start()
+            att[t % 2 * NZ + t // 2] = (acc_ref[span, :HD] / acc_ref[span, HD:]).astype(BF16)
+        for dz in range(NZ):
+            if dz > 0:
+                att_copy(dz, c).start()
+            att_copy(dz, sib).start()
+        att_all[c, :, pl.ds(pl.multiple_of(z * HD, HD), HD)] = att[c * NZ + z]
 
     piece = HALF // RSUBS
 
@@ -387,20 +431,13 @@
         step = 1 if way == 0 else -1
         return remote(
             rs_buf.at[way, s, u], rs_buf.at[way, s + 1, u],
-            rs_send.at[way, s, u], rs_recv.at[way, s, u], z=(z + step) % NZ,
-        )
-
-    def ars_copy(way, s):
-        step = 1 if way == 0 else -1
-        return remote(
-            ars_buf.at[way, s], ars_buf.at[way, s + 1],
-            ars_send.at[way, s], ars_recv.at[way, s], z=(z + step) % NZ,
+            ring_sent.at[way], rs_recv.at[way, s, u], z=(z + step) % NZ,
         )
 
     def ret_copy(p):
         dy, dx = OWNERS[p]
         return remote(
-            fin.at[p], ret.at[me], ret_send.at[p], ret_recv.at[p],
+            fin.at[p], ret.at[me], sent.at[3], sent.at[4],
             y=(y + dy) % NY, x=(x + dx) % NX,
         )
 
@@ -412,7 +449,7 @@
                     for copy in awaited:
                         copy.wait_recv()
                 elif k < REACH:
-                    for sub in range(SUBS):
+                    for sub in SUB_ORDER:
                         z_forward(k, sub)
                 else:
                     for delta in sorted({k + 1, NZ - k - 1}):
@@ -465,39 +502,6 @@
                             if p != SELF:
                                 ret_copy(p).start()
 
-    def att_step(s):
-        @pl.when(s == 0)
-        def _():
-            swap_att.wait_recv()
-
-        chunk_r = (z - 1 - s + 2 * NZ) % NZ
-        chunk_l = (z + 1 + s) % NZ
-        for way, chunk in ((0, chunk_r), (1, chunk_l)):
-            cols = pl.ds(way * (D // 2), D // 2)
-            ap[way] = jnp.dot(att[c, chunk], ow[c, :, cols], preferred_element_type=F32) + jnp.dot(
-                att_sib[chunk], ow[sib, :, cols], preferred_element_type=F32
-            )
-
-        for way in (0, 1):
-            @pl.when(s == 0)
-            def _(way=way):
-                ars_buf[way, 0] = ap[way].astype(BF16)
-                ars_copy(way, 0).start()
-
-            @pl.when(s > 0)
-            def _(way=way):
-                ars_copy(way, s - 1).wait_recv()
-                total = ap[way] + ars_buf[way, s].astype(F32)
-
-                @pl.when(s < NZ - 1)
-                def _():
-                    ars_buf[way, s] = total.astype(BF16)
-                    ars_copy(way, s).start()
-
-                @pl.when(s == NZ - 1)
-                def _():
-                    out_ref[0, :, way * (D // 2) : (way + 1) * (D // 2)] = total.astype(BF16)
-
     def tick(t, carry):
         @pl.when(t < UNITS)
         def _():
@@ -507,57 +511,60 @@
         def _():
             finish_attention()
 
-        @pl.when((t == EARLY) | ((t >= UNITS) & (t < UNITS + NZ - 1)))
+        @pl.when((t == EARLY[0]) | (t == EARLY[1]) | ((t >= UNITS) & (t < UNITS + NZ - len(EARLY))))
         def _():
-            moe_step(jnp.where(t == EARLY, 0, t - UNITS + 1))
-
-        @pl.when(t >= UNITS)
-        def _():
-            att_step(t - UNITS)
+            moe_step(
+                jnp.where(t == EARLY[0], 0, jnp.where(t == EARLY[1], 1, t - UNITS + len(EARLY)))
+            )
+
+        for at, level in late.items():
+            @pl.when(t == at)
+            def _(level=level):
+                wos.level(level)
 
         return carry
 
-    lax.fori_loop(0, UNITS + NZ, tick, 0)
-
+    lax.fori_loop(0, TICKS, tick, 0)
+
+    own = wo.at[sib, 0]
+    remote(own, own, d2d_send.at[3], d2d_recv.at[3], c=sib).wait_recv()
+    for pair in range(NE // 2):
+        wos.wait(pair)
+    heads = att.at[pl.ds(0, 2 * NZ - 1)]
+    remote(heads, heads, sent.at[9], sent.at[10], c=sib).wait_recv()
+    for slot, (dy, dx) in enumerate(PLACES):
+        owner = (y + dy) % NY * NX + (x + dx) % NX
+        cols = pl.ds(pl.multiple_of(owner * HD, HD), HD)
+        stage[0, :, cols] = (
+            jnp.dot(att_all[0], wo[0, slot], preferred_element_type=F32)
+            + jnp.dot(att_all[1], wo[1, slot], preferred_element_type=F32)
+        ).astype(BF16)
+    outs[0].start()
     ret[me] = fin[SELF]
-    own = 2 * z + c
-    j = lax.broadcasted_iota(jnp.int32, (CH, TOK), 0)
-    picks = block_of(routes_ref, own)
-    sizes = block_of(sizes_ref, own)
-    w0, w1 = sizes[0:1], sizes[1:2]
-    share = jnp.where(picks[0:1] == j // CAP, w0, w1) / (w0 + w1)
-    combine = jnp.where(mat_ref[...] > 0.5, share, 0.0)
-    high = combine.astype(BF16)
-    low = (combine - high.astype(F32)).astype(BF16)
-    for p in OTHERS:
-        ret_copy(p).wait_recv()
+    got = ret.at[pl.ds(0, NE - 1)]
+    remote(got, got, sent.at[3], sent.at[4], c=sib).wait_recv()
     back = ret[...].reshape(CH, D)
     dims = (((0,), (0,)), ((), ()))
-    out_ref[1] = (
-        lax.dot_general(high, back, dims, preferred_element_type=F32)
-        + lax.dot_general(low, back, dims, preferred_element_type=F32)
+    stage[1] = (
+        lax.dot_general(comb[0], back, dims, preferred_element_type=F32)
+        + lax.dot_general(comb[1], back, dims, preferred_element_type=F32)
     ).astype(BF16)
-
-    for p in OTHERS:
-        ret_copy(p).wait_send()
-    for n in range(N_MSG):
-        kv_copy(n).wait_send()
-    for slot in range(1, NE):
-        for half in (0, 1):
-            kv_across(slot, half).wait_send()
-    for i in range(len(DIRECT)):
-        for p in OTHERS:
-            a2a(i, p).wait_send()
+    outs[1].start()
+
+    for span, sem in (
+        [(fin.at[pl.ds(0, NE - 1)], sent.at[3]), (rows.at[pl.ds(0, 2 * REACH)], sent.at[2])]
+        + [(kv.at[c, pl.ds(1, NE - 1)], sent.at[k]) for k in (0, 1)]
+        + [(slots.at[i, pl.ds(0, NE - 1)], a2a_sent.at[i]) for i in range(len(DIRECT))]
+        + [(rs_buf.at[way, pl.ds(0, NZ - 1)], ring_sent.at[way]) for way in (0, 1)]
+        + [(wo.at[c, pl.ds(1, NE - 1)], sent.at[k]) for k in (5, 6)]
+        + [(wo.at[c, 0, pl.ds(0, WO_ROWS - HD)], sent.at[7]), (heads, sent.at[9])]
+        + [(wo.at[c, 0], d2d_send.at[3])]
+    ):
+        remote(span, span, sem, sent.at[4], c=sib).wait_send()
     for copy in pairs:
         copy.wait_send()
-    swap_att.wait_send()
-    for way in (0, 1):
-        for hop, sub in hops:
-            z_copy(way, hop, sub).wait_send()
-        for s in range(NZ - 1):
-            for u in range(RSUBS):
-                rs_copy(way, s, u).wait_send()
-            ars_copy(way, s).wait_send()
+    for copy in outs:
+        copy.wait()
 
 
 def fused(*args):
@@ -570,7 +577,7 @@
         name="fused_step",
         out_shape=jax.ShapeDtypeStruct((2, TOK, D), BF16),
         in_specs=[hbm] * 3 + [vmem] * 6 + [hbm] * 5,
-        out_specs=vmem,
+        out_specs=hbm,
         scratch_shapes=[
             pltpu.VMEM((ROWS, HD), BF16),
             pltpu.VMEM((ROWS, HD), BF16),
@@ -579,30 +586,26 @@
             pltpu.VMEM((ROWS, HD), BF16),
             pltpu.VMEM((ROWS, HD), F32),
             pltpu.VMEM((ROWS, 2 * HD), F32),
-            pltpu.VMEM((2, NZ, TOK, HD), BF16),
-            pltpu.VMEM((NZ, TOK, HD), BF16),
+            pltpu.VMEM((2 * NZ, TOK, HD), BF16),
             pltpu.VMEM((n_direct, NE, CAP, D), BF16),
             pltpu.VMEM((NZ, NE, CAP, D), BF16),
             pltpu.VMEM((2, D, FF_DEV), BF16),
             pltpu.VMEM((2, D, FF_DEV), BF16),
             pltpu.VMEM((2, FF_DEV, D), BF16),
-            pltpu.VMEM((2, HD, D), BF16),
+            pltpu.VMEM((2, NE, WO_ROWS, HD), BF16),
+            pltpu.VMEM((2, TOK, WO_ROWS), BF16),
             pltpu.VMEM((CH, D), F32),
             pltpu.VMEM((2, NZ, RSUBS, HALF // RSUBS, D), BF16),
-            pltpu.VMEM((2, TOK, D // 2), F32),
-            pltpu.VMEM((2, NZ, TOK, D // 2), BF16),
             pltpu.VMEM((NE, CAP, D), BF16),
             pltpu.VMEM((NE, CAP, D), BF16),
             pltpu.VMEM((CH, TOK), F32),
+            pltpu.VMEM((2, CH, TOK), BF16),
+            pltpu.VMEM((2, TOK, D), BF16),
             dma((3 + n_direct + 4,)),
-            dma((5,)), dma((5,)),
-            dma((N_MSG,)), dma((N_MSG,)),
-            dma((2 * NE - 2,)), dma((2 * NE - 2,)),
-            dma((n_direct, NE)), dma((n_direct, NE)),
-            dma((2, REACH, SUBS)), dma((2, REACH, SUBS)),
-            dma((2, NZ, RSUBS)), dma((2, NZ, RSUBS)),
-            dma((2, NZ)), dma((2, NZ)),
-            dma((NE,)), dma((NE,)),
+            dma((4,)), dma((4,)),
+            dma((11,)), dma((n_direct,)), dma((2,)),
+            dma((2 * NE - 2,)), dma((UNITS,)), dma((SUBS + n_direct - 1,)), dma((2, REACH, SUBS)),
+            dma((2 * NE - 2,)), dma((UNITS,)), dma((2, NZ - 1, RSUBS)), dma((2,)),
         ],
         compiler_params=pltpu.CompilerParams(
             collective_id=0, has_side_effects=True, vmem_limit_bytes=60 * 2**20

time: 111 us -> 101 us (0.910); the launches traced: 109 us -> 101 us
  Pallas kernels: 107 us -> 98.7 us
    pallas_call x1, Pallas kernels: 107 us -> 98.7 us  [fused(): pl.pallas_call(body, name='fused_step', out_shape=jax.ShapeDtypeStruct((2...]
where the time goes in v3:
time: 101 us
  Pallas kernels  98.7 us (98%)
  local copies, waits for them, and re-layouts  1.79 us (2%)
    pallas_call x1, Pallas kernels, fused(): pl.pallas_call(body, name='fused_step', out_shape=jax.ShapeDtypeStruct((2...  98.7 us

profile of v3, /device:TPU:4, one launch (start us, length us, event | category | flops | bytes accessed | tf_op | source)
XLA Modules:
  0.0 101.1 jit_solution(10446371563745665484)
XLA Ops:
  0.6 98.7 %fused_step.1 = bf16[2,48,2048]{2,1,0:T(8,128)(2,1)} custom-call(bf16[768,128]{1,0:T(8,128)(2,1)} %q_hbm.1, bf16[768,512]{1,0:T(8,128)(2,1)} %k_hbm.1, bf16[768,512]{1,0:T(8,128)(2,1)} %v_hbm.1, f32[1,128]{1,0:T(1,128)} %bitcast.18, f32[1,128]{1,0:T(1,128)} %bitcast.19, f32[1,128]{1,0:T(1,128)} %constant.6.inv_ref, f32[1,2048]{1,0:T(1,128)} %bitcast.15, ...), custom_call_target="tpu_custom_call" | custom-call | tf_op jit(solution)/shard_map/fused_step/pallas_call | solution.py:575
  99.3 1.8 %slice_bitcast_fusion = (bf16[48,2048]{1,0:T(8,128)(2,1)}, bf16[48,2048]{1,0:T(8,128)(2,1)}) fusion(bf16[2,48,2048]{2,1,0:T(8,128)(2,1)} %fused_step.1), kind=kLoop, calls=%fused_computation | loop fusion | bytes 786432 | tf_op jit(solution)/shard_map/squeeze | solution.py:627

commit v4 on v3

--- a/solution.py
+++ b/solution.py
@@ -302,7 +302,6 @@
     kvs = Gather(kv, ROWS, 0, kv_recv, kvd_recv)
     wos = Gather(wo, WO_ROWS, 5, wo_recv, wod_recv)
     kv_level = kvs.level
-    kvs.start()
 
     def wo_copy(dz):
         return remote(wo_own, wo_own, sent.at[7], sent.at[8], z=(z + dz) % NZ)
@@ -354,6 +353,8 @@
     def z_start():
         for sub in SUB_ORDER:
             wait_own(sub)
+            if sub == SUB_ORDER[1]:
+                kvs.start()
             for way in (0, 1):
                 z_copy(way, 0, sub).start()
 
@@ -381,7 +382,7 @@
     plan[2] += [functools.partial(start_direct, 1)]
     plan[4] += [functools.partial(kv_level, 3), functools.partial(start_direct, 3)]
     plan[6] += [functools.partial(kv_level, 4), functools.partial(start_direct, 2), wo_start]
-    late = {UNITS: 1, UNITS + 2: 2, UNITS + 3: 3, UNITS + 4: 4}
+    late = {UNITS: 1, UNITS + 2: 2, UNITS + 3: 3}
 
     def unit(u):
         for k in range(UNITS):
@@ -528,6 +529,7 @@
 
     own = wo.at[sib, 0]
     remote(own, own, d2d_send.at[3], d2d_recv.at[3], c=sib).wait_recv()
+    wos.level(4)
     for pair in range(NE // 2):
         wos.wait(pair)
     heads = att.at[pl.ds(0, 2 * NZ - 1)]

time: 101 us -> 98.8 us (0.978); the launches traced: 101 us -> 97.4 us
  Pallas kernels: 98.7 us -> 95 us
    pallas_call x1, Pallas kernels: 98.7 us -> 95 us  [fused(): pl.pallas_call(body, name='fused_step', out_shape=jax.ShapeDtypeStruct((2...]
where the time goes in v4:
time: 98.8 us; the launch traced here: 97.4 us
  Pallas kernels  95 us (96%)
  local copies, waits for them, and re-layouts  1.79 us (2%)
    pallas_call x1, Pallas kernels, fused(): pl.pallas_call(body, name='fused_step', out_shape=jax.ShapeDtypeStruct((2...  95 us

profile of v4, /device:TPU:4, one launch (start us, length us, event | category | flops | bytes accessed | tf_op | source)
XLA Modules:
  0.0 97.4 jit_solution(15148168851504676750)
XLA Ops:
  0.6 95.0 %fused_step.1 = bf16[2,48,2048]{2,1,0:T(8,128)(2,1)} custom-call(bf16[768,128]{1,0:T(8,128)(2,1)} %q_hbm.1, bf16[768,512]{1,0:T(8,128)(2,1)} %k_hbm.1, bf16[768,512]{1,0:T(8,128)(2,1)} %v_hbm.1, f32[1,128]{1,0:T(1,128)} %bitcast.18, f32[1,128]{1,0:T(1,128)} %bitcast.19, f32[1,128]{1,0:T(1,128)} %constant.6.inv_ref, f32[1,2048]{1,0:T(1,128)} %bitcast.15, ...), custom_call_target="tpu_custom_call" | custom-call | tf_op jit(solution)/shard_map/fused_step/pallas_call | solution.py:577
  95.6 1.8 %slice_bitcast_fusion = (bf16[48,2048]{1,0:T(8,128)(2,1)}, bf16[48,2048]{1,0:T(8,128)(2,1)}) fusion(bf16[2,48,2048]{2,1,0:T(8,128)(2,1)} %fused_step.1), kind=kLoop, calls=%fused_computation | loop fusion | bytes 786432 | tf_op jit(solution)/shard_map/squeeze | solution.py:629
